TPU v7x, 256 devices: a 4x2x16 block of a 4x16x16 slice. The times are simulated.
256 devices in a mesh: grp: 2 (over y), sp: 32 (over z, core), tp: 4 (over x).
Axes of the slice: x: 4, y: 2, z: 16, core: 2. Of those that a mesh axis runs over, the one named last changes fastest.
The devices are a block of a 4x16x16 slice.
Arguments:
- residual: bfloat16 [45056, 2048], P(('grp', 'sp')), parts along dimension 0, may hold values from -6 to 6
- mix_input: bfloat16 [45056, 2048], P(('grp', 'sp'), 'tp'), parts along dimension 0, may hold values from -6 to 6
- gate_input: bfloat16 [45056, 2048], P(('grp', 'sp'), 'tp'), parts along dimension 0, may hold values from -6 to 6
- mix_kernel: bfloat16 [4, 2048], P(None, 'tp'), may hold values from -3 to 3
- recur_gate_map: bfloat16 [16, 128, 128], P('tp'), may hold values from -0.5 to 0.5
- input_gate_map: bfloat16 [16, 128, 128], P('tp'), may hold values from -0.5 to 0.5
- decay_param: float32 [2048], P('tp')
- jump_log: float32 [45056, 2048], P(('grp', 'sp'), 'tp'), parts along dimension 0, may hold values from -2.1 to 0
- out_weight: bfloat16 [2048, 2048], P('tp'), may hold values from -0.125 to 0.125
- mix_gain: float32 [2048], replicated, may hold values from 0.1 to 1.9
- inner_gain: float32 [2048], replicated, may hold values from 0.1 to 1.9
- final_gain: float32 [2048], replicated, may hold values from 0.1 to 1.9
- gate_weight: bfloat16 [2048, 5632], P('sp', 'tp'), may hold values from -0.125 to 0.125
- value_weight: bfloat16 [2048, 5632], P('sp', 'tp'), may hold values from -0.125 to 0.125
- gate_kernel: bfloat16 [3, 5632], P(None, 'tp'), may hold values from -3.5 to 3.5
- value_kernel: bfloat16 [3, 5632], P(None, 'tp'), may hold values from -3.5 to 3.5
- down_weight: bfloat16 [5632, 2048], P('tp', 'sp'), may hold values from -0.078125 to 0.078125
Outputs:
- layer_output: bfloat16 [45056, 2048], P(('grp', 'sp', 'tp')), parts along dimension 0
There are 2 independent parts, one for each index of `grp`. A program takes and returns all parts, laid end to end along the dimension named above; an argument that names none is the same for every part. Nothing has to cross between parts.
All inputs are finite; a program needn't handle non-finite values.
Results may differ from a plain program's by a relative error of at most 0.02.
Values may be sent and summed in bfloat16 or wider, within the bound.
A program may use at most 128 MiB of HBM per device.

v0:
```python
import jax
import jax.numpy as jnp
from jax import lax
from jax.sharding import PartitionSpec as P

EPS = 1e-06
GATE_SCALE = 8.0


def turned_gather(arrays, axis, dims):
    turned = [jnp.moveaxis(a, dim, 0) for a, dim in zip(arrays, dims)]
    widths = [t[0].size for t in turned]
    both = jnp.concatenate([t.reshape(-1, w) for t, w in zip(turned, widths)], axis=1)
    filled = lax.all_gather(both, axis, axis=0, tiled=True)
    tiles = jnp.split(filled, [sum(widths[:k]) for k in range(1, len(widths))], axis=1)
    return tuple(
        (
            jnp.moveaxis(b.reshape(-1, *t.shape[1:]), 0, dim)
            for b, t, dim in zip(tiles, turned, dims)
        )
    )


def from_behind(value, axis, steps):
    count = lax.axis_size(axis)
    initial, last = (max(0, -steps), min(count, count - steps))
    return lax.ppermute(value, axis, [(source, source + steps) for source in range(initial, last)])


def copy_for_each(shard, axis):
    copies = jnp.broadcast_to(shard, (lax.axis_size(axis), *shard.shape))
    return lax.all_to_all(copies, axis, split_axis=0, concat_axis=0, tiled=True)


def collected_together(shard, axis):
    leaves = jax.tree.leaves(shard)
    order = sorted(range(len(leaves)), key=lambda k: -leaves[k].size)
    width = (1, *leaves[order[0]].shape)[-1]
    lines = [
        jnp.pad(leaves[k].reshape(-1), (0, -leaves[k].size % width)).reshape(-1, width)
        for k in order
    ]
    both, at, found = (copy_for_each(jnp.concatenate(lines), axis), 0, {})
    for k, line in zip(order, lines):
        share = both[:, at : at + len(line)].reshape(len(both), -1)
        found[k] = share[:, : leaves[k].size].reshape(-1, *leaves[k].shape)
        at += len(line)
    numbers = iter(range(len(leaves)))
    return jax.tree.map(lambda _: found[next(numbers)], shard)


def joined_by_halves(pieces, combine):
    while len(jax.tree.leaves(pieces)[0]) > 1:
        pieces = jax.vmap(combine)(
            *(jax.tree.map(lambda part: part[side::2], pieces) for side in (0, 1))
        )
    return jax.tree.map(lambda part: part[0], pieces)


def prefix(shard, axis, combine, identity):
    size, index = (lax.axis_size(axis), lax.axis_index(axis))
    passed = jnp.arange(size) < index

    def kept(part, zero, own):
        part = jnp.where(
            passed.reshape(-1, *(1 for _ in own.shape)), part, jnp.asarray(zero, own.dtype)
        )
        return part

    pieces = collected_together(shard, axis)
    return joined_by_halves(jax.tree.map(kept, pieces, identity, shard), combine)


def in_blocks(shard, dim, size):
    before, after = (shard.shape[:dim], shard.shape[dim + 1 :])
    return jnp.moveaxis(shard.reshape(*before, size, -1, *after), dim, 0)


def summed_on_arrival(shard, axis, dim):
    tiles = in_blocks(shard, dim, lax.axis_size(axis))
    arrived = lax.all_to_all(tiles, axis, split_axis=0, concat_axis=0, tiled=True)
    return arrived.astype(jnp.float32).sum(axis=0)


def laid_out(tiles, dim):
    lengths = list(tiles.shape[1:])
    lengths[dim] *= tiles.shape[0]
    return jnp.moveaxis(tiles, 0, dim).reshape(lengths)


def gather_directly(shard, axis, dim):
    return laid_out(copy_for_each(shard, axis), dim)


def norm_scale(values, gain_vec):
    values = values.astype(jnp.float32)
    return values * lax.rsqrt(jnp.mean(values * values, axis=-1, keepdims=True) + EPS) * gain_vec


def causal_taps(padded, kernel, length):
    kernel = kernel.astype(jnp.float32)
    result = jnp.zeros((length, padded.shape[1]), jnp.float32)
    for offset in range(kernel.shape[0]):
        result = result + padded[offset : offset + length] * kernel[offset]
    return result


def linear_pair(before_pair, after_pair):
    return (before_pair[0] * after_pair[0], after_pair[0] * before_pair[1] + after_pair[1])


def rounded(values):
    return lax.optimization_barrier(values.astype(jnp.bfloat16)).astype(jnp.float32)


def local(
    residual,
    mix_input,
    gate_input,
    mix_kernel,
    recur_gate_map,
    input_gate_map,
    decay_param,
    jump_log,
    out_weight,
    mix_gain,
    inner_gain,
    final_gain,
    gate_weight,
    value_weight,
    gate_kernel,
    value_kernel,
    down_weight,
):
    length = mix_input.shape[0]
    row_share = length // lax.axis_size("tp")
    column_index = lax.axis_index("tp")
    gate_whole, value_whole, down_whole = turned_gather(
        (gate_weight, value_weight, down_weight), "sp", (0, 0, 1)
    )
    mix_taps = mix_kernel.shape[0]
    mix_edge = from_behind(mix_input[length - mix_taps + 1 :], "sp", 1)
    padded = jnp.concatenate([mix_edge, mix_input], axis=0).astype(jnp.float32)
    conv_rows = causal_taps(padded, mix_kernel, length).astype(jnp.bfloat16)
    groups = recur_gate_map.shape[0]
    block_width = recur_gate_map.shape[1]
    grouped = conv_rows.reshape(length, groups, block_width)
    recur_gate = jax.nn.sigmoid(
        jnp.einsum("tnd,nde->tne", grouped, recur_gate_map, preferred_element_type=jnp.float32)
    ).reshape(length, groups * block_width)
    input_gate = jax.nn.sigmoid(
        jnp.einsum("tnd,nde->tne", grouped, input_gate_map, preferred_element_type=jnp.float32)
    ).reshape(length, groups * block_width)
    log_decay = -GATE_SCALE * recur_gate * jax.nn.softplus(-decay_param) + jump_log
    drive = jnp.sqrt(-jnp.expm1(2.0 * log_decay)) * input_gate * conv_rows.astype(jnp.float32)
    cumulative, local_state = lax.associative_scan(linear_pair, (jnp.exp(log_decay), drive), axis=0)
    block_end = (cumulative[length - 1], local_state[length - 1])
    carried = prefix(
        block_end, "sp", linear_pair, (jnp.ones_like(block_end[0]), jnp.zeros_like(block_end[1]))
    )
    state = local_state + cumulative * carried[1]
    branch = (state * jax.nn.gelu(gate_input.astype(jnp.float32), approximate=True)).astype(
        jnp.bfloat16
    )
    chosen = branch
    mixed = summed_on_arrival(
        rounded(jnp.dot(chosen, out_weight, preferred_element_type=jnp.float32)).astype(
            jnp.bfloat16
        ),
        "tp",
        0,
    ).astype(jnp.bfloat16)
    own_rows = lax.dynamic_slice_in_dim(residual, column_index * row_share, row_share, 0)
    hidden_state = (own_rows.astype(jnp.float32) + norm_scale(mixed, mix_gain)).astype(jnp.bfloat16)
    normed = gather_directly(norm_scale(hidden_state, inner_gain).astype(jnp.bfloat16), "tp", 0)
    up_gate = jnp.dot(normed, gate_whole, preferred_element_type=jnp.float32).astype(jnp.bfloat16)
    up_value = jnp.dot(normed, value_whole, preferred_element_type=jnp.float32).astype(jnp.bfloat16)
    hidden_taps = gate_kernel.shape[0]
    tails = jnp.stack([up_gate[length - hidden_taps + 1 :], up_value[length - hidden_taps + 1 :]])
    hidden_edge = from_behind(tails, "sp", 1)
    gate_conv = causal_taps(
        jnp.concatenate([hidden_edge[0], up_gate], axis=0).astype(jnp.float32), gate_kernel, length
    )
    value_conv = causal_taps(
        jnp.concatenate([hidden_edge[1], up_value], axis=0).astype(jnp.float32),
        value_kernel,
        length,
    )
    activation = (jax.nn.gelu(gate_conv, approximate=True) * value_conv).astype(jnp.bfloat16)
    chosen = activation
    down_sum = summed_on_arrival(
        rounded(jnp.dot(chosen, down_whole, preferred_element_type=jnp.float32)).astype(
            jnp.bfloat16
        ),
        "tp",
        0,
    )
    down = down_sum.astype(jnp.bfloat16)
    return (hidden_state.astype(jnp.float32) + norm_scale(down, final_gain)).astype(jnp.bfloat16)


def solution(mesh):
    return jax.shard_map(
        local,
        mesh=mesh,
        in_specs=(
            P(("grp", "sp"), None),
            P(("grp", "sp"), "tp"),
            P(("grp", "sp"), "tp"),
            P(None, "tp"),
            P("tp", None, None),
            P("tp", None, None),
            P("tp"),
            P(("grp", "sp"), "tp"),
            P("tp", None),
            P(),
            P(),
            P(),
            P("sp", "tp"),
            P("sp", "tp"),
            P(None, "tp"),
            P(None, "tp"),
            P("tp", "sp"),
        ),
        out_specs=P(("grp", "sp", "tp"), None),
        check_vma=False,
    )
```

profile of v0, /device:TPU:33, one launch (start us, length us, event | category | flops | bytes accessed | tf_op | source)
XLA Modules:
  0.0 335.7 jit_solution(13415458491723378446)
XLA Ops:
  6.6 2.2 pad_maximum_fusion.2
  8.9 5.7 %collective-permute-start = (bf16[3,512]{1,0:T(4,128)(2,1)S(1)}, bf16[3,512]{1,0:T(4,128)(2,1)S(1)}, u32[]{:S(2)}, u32[]{:S(2)}) collective-permute-start(bf16[3,512]{1,0:T(4,128)(2,1)S(1)} %slice.393), channel_id=1, source_target_pairs={{0,4},{4,8},{8,12},{12,16},{16,20},{20,24},{24,28},{28,32},{32,36}... | collective-permute-start | bytes 9224 | tf_op jit(solution)/shard_map/ppermute | solution.py:27
  14.7 16.6 %collective-permute-done = bf16[3,512]{1,0:T(4,128)(2,1)S(1)} collective-permute-done((bf16[3,512]{1,0:T(4,128)(2,1)S(1)}, bf16[3,512]{1,0:T(4,128)(2,1)S(1)}, u32[]{:S(2)}, u32[]{:S(2)}) %collective-permute-start) | collective-permute-done | bytes 3104 | tf_op jit(solution)/shard_map/ppermute | solution.py:27
  34.6 2.8 fusion.64
  38.2 4.9 %slice.466 = f32[351,512]{1,0:T(8,128)} slice(f32[704,512]{1,0:T(8,128)} %get-tuple-element.17), slice={[2:704:2], [0:512:1]} | slice | bytes 1437696 | tf_op jit(solution)/shard_map/slice | solution.py:156
  43.0 4.7 %slice.406 = f32[352,512]{1,0:T(8,128)} slice(f32[704,512]{1,0:T(8,128)} %get-tuple-element.17), slice={[1:704:2], [0:512:1]} | slice | bytes 1441792 | tf_op jit(solution)/shard_map/slice | solution.py:156
  47.8 4.7 %slice.405 = f32[352,512]{1,0:T(8,128)} slice(f32[704,512]{1,0:T(8,128)} %get-tuple-element.17), slice={[0:703:2], [0:512:1]} | slice | bytes 1441792 | tf_op jit(solution)/shard_map/slice | solution.py:156
  52.5 2.7 slice.408
  55.2 2.7 slice.404
  58.0 2.8 slice.403
  60.7 2.1 multiply_add_fusion
  62.8 1.5 slice.464
  64.3 1.4 slice.412
  65.7 1.4 slice.411
  67.2 1.4 slice.414
  68.6 1.4 slice.410
  70.0 1.5 slice.409
  71.5 1.2 multiply_add_fusion.1
  79.2 1.0 pad.141
  81.8 1.0 fusion.82
  82.9 0.8 copy-done.13
  84.5 1.1 pad.124
  85.7 2.8 pad.125
  88.5 2.8 pad.143
  91.3 2.2 add.323
  93.5 1.0 add.313
  95.3 1.4 fusion.73
  96.8 3.1 pad.144
  100.0 3.0 pad.126
  103.0 3.1 pad.127
  106.1 3.0 pad.145
  109.1 0.9 slice_add_fusion.1
  111.4 8.1 %all-to-all-start = ((f32[32,2,512]{2,1,0:T(2,128)}), f32[32,2,512]{2,1,0:T(2,128)}, u32[]{:S(2)}, u32[]{:S(2)}) async-start(f32[32,2,512]{2,1,0:T(2,128)} %broadcast_in_dim.34), calls=%async_computation | async-start | bytes 262144 | tf_op jit(solution)/shard_map/all_to_all | solution.py:32
  119.5 18.0 %all-to-all-done = f32[32,2,512]{2,1,0:T(2,128)} async-done(((f32[32,2,512]{2,1,0:T(2,128)}), f32[32,2,512]{2,1,0:T(2,128)}, u32[]{:S(2)}, u32[]{:S(2)}) %all-to-all-start) | async-done | bytes 131104 | tf_op jit(solution)/shard_map/all_to_all | solution.py:32
  137.5 1.1 fusion.100
  139.3 1.5 slice.486
  140.8 1.4 slice.485
  142.2 1.5 slice.496
  143.7 1.5 slice.495
  145.1 1.4 fusion.101
  146.6 1.4 slice.488
  147.9 1.4 slice.487
  149.3 1.4 slice.498
  150.7 1.4 slice.497
  152.0 1.4 fusion.102
  153.4 1.3 slice.490
  154.7 1.3 slice.489
  160.7 6.1 %convolution_convert_fusion = bf16[704,2048]{1,0:T(8,128)(2,1)} fusion(bf16[512,2048]{1,0:T(8,128)(2,1)S(1)} %copy-done, bf16[704,512]{1,0:T(8,128)(2,1)} %param.19, f32[704,512]{1,0:T(8,128)S(1)} %copy-done.9, f32[704,512]{1,0:T(8,128)} %pad.145, f32[704,512]{1,0:T(8,128)} %pad.126, f32[704,512]{1,0:T(8,128)} %pad.127, f32[512]{0:T(512)S(1)} %bitcast.64), kind=kOutput, calls=%fused_computation.26 | convolution fusion | flops 1483243520 | bytes 11470848 | tf_op jit(solution)/shard_map/dot_general | solution.py:167
  166.7 4.3 %all-to-all-start.1 = ((bf16[4,176,2048]{2,1,0:T(8,128)(2,1)}), bf16[4,176,2048]{2,1,0:T(8,128)(2,1)S(1)}, u32[]{:S(2)}, u32[]{:S(2)}) async-start(bf16[4,176,2048]{2,1,0:T(8,128)(2,1)} %bitcast.53), calls=%async_computation.1 | async-start | bytes 5767168 | tf_op jit(solution)/shard_map/all_to_all | solution.py:81
  171.0 33.6 %all-to-all-done.1 = bf16[4,176,2048]{2,1,0:T(8,128)(2,1)S(1)} async-done(((bf16[4,176,2048]{2,1,0:T(8,128)(2,1)}), bf16[4,176,2048]{2,1,0:T(8,128)(2,1)S(1)}, u32[]{:S(2)}, u32[]{:S(2)}) %all-to-all-start.1) | async-done | bytes 2883616 | tf_op jit(solution)/shard_map/all_to_all | solution.py:81
  204.6 1.6 reduce_sum.51
  206.2 1.3 fusion.47
  207.5 1.8 fusion.53
  209.6 2.0 broadcast_in_dim.37
  211.6 4.9 %all-to-all-start.2 = ((bf16[4,176,2048]{2,1,0:T(8,128)(2,1)}), bf16[4,176,2048]{2,1,0:T(8,128)(2,1)}, u32[]{:S(2)}, u32[]{:S(2)}) async-start(bf16[4,176,2048]{2,1,0:T(8,128)(2,1)} %broadcast_in_dim.37), calls=%async_computation.2 | async-start | bytes 5767168 | tf_op jit(solution)/shard_map/all_to_all | solution.py:32
  216.5 32.7 %all-to-all-done.2 = bf16[4,176,2048]{2,1,0:T(8,128)(2,1)} async-done(((bf16[4,176,2048]{2,1,0:T(8,128)(2,1)}), bf16[4,176,2048]{2,1,0:T(8,128)(2,1)}, u32[]{:S(2)}, u32[]{:S(2)}) %all-to-all-start.2) | async-done | bytes 2883616 | tf_op jit(solution)/shard_map/all_to_all | solution.py:32
  249.2 8.3 %fusion.19 = bf16[704,1408]{1,0:T(8,128)(2,1)S(1)} fusion(bf16[704,2048]{1,0:T(8,128)(2,1)} %bitcast.9, bf16[2048,4224]{1,0:T(8,128)(2,1)} %all-gather.2.cloned.1.call-done), kind=kOutput, calls=%fused_computation.27 | convolution fusion | flops 4061077504 | bytes 10633216 | tf_op jit(solution)/shard_map/dot_general | solution.py:176
  257.6 6.5 %fusion.22 = bf16[704,1408]{1,0:T(8,128)(2,1)S(1)} fusion(bf16[704,2048]{1,0:T(8,128)(2,1)} %bitcast.9, bf16[2048,4224]{1,0:T(8,128)(2,1)S(1)} %copy-done.25), kind=kOutput, calls=%fused_computation.28 | convolution fusion | flops 4061077504 | bytes 10633216 | tf_op jit(solution)/shard_map/dot_general | solution.py:177
  264.1 4.4 %collective-permute-start.1 = (bf16[2,2,1408]{2,1,0:T(2,128)(2,1)S(1)}, bf16[2,2,1408]{2,1,0:T(2,128)(2,1)S(1)}, u32[]{:S(2)}, u32[]{:S(2)}) collective-permute-start(bf16[2,2,1408]{2,1,0:T(2,128)(2,1)S(1)} %pad_maximum_fusion.15), channel_id=1, source_target_pairs={{0,4},{4,8},{8,12},{12,16},{16,20},{20,24},{24,28},{28,32},{32,36}... | collective-permute-start | bytes 33800 | tf_op jit(solution)/shard_map/ppermute | solution.py:27
  269.5 2.3 maximum_convert_fusion.1
  271.8 13.3 %fusion.25 = bf16[704,2048]{1,0:T(8,128)(2,1)} fusion(bf16[2048,4224]{1,0:T(8,128)(2,1)} %all-gather.2.cloned.1.call-done, f32[706,1408]{1,0:T(8,128)} %maximum_convert_fusion.1, f32[706,1408]{1,0:T(8,128)S(1)} %maximum_convert_fusion, f32[1408]{0:T(1024)S(1)} %get-tuple-element.9, f32[1408]{0:T(1024)S(1)} %get-tuple-element.10, ...), kind=kOutput, calls=%fused_computation.29 | convolution fusion | flops 4081352704 | bytes 32489472 | tf_op jit(solution)/shard_map/dot_general | solution.py:192
  285.2 39.6 %all_to_all.20 = bf16[4,176,2048]{2,1,0:T(8,128)(2,1)} all-to-all(bf16[4,176,2048]{2,1,0:T(8,128)(2,1)} %bitcast.54), channel_id=1, replica_groups=mesh['grp'=2,'sp'=32,'tp'=4] {'tp'}, dimensions={0} | all-to-all | bytes 5767168 | tf_op jit(solution)/shard_map/all_to_all | solution.py:81
  324.8 2.6 reduce_sum.54
  327.6 1.3 fusion.56
  (207 shorter events, 22.0 us)
Async XLA Ops:
  6.5 154.1 %copy-start = (bf16[512,2048]{1,0:T(8,128)(2,1)S(1)}, bf16[512,2048]{1,0:T(8,128)(2,1)}, u32[]{:S(2)}) copy-start(bf16[512,2048]{1,0:T(8,128)(2,1)} %param.25) | copy-start | bytes 6291460
  6.6 2.3 copy-start.16
  6.6 8.1 %copy-start.17 = (bf16[4,512]{1,0:T(4,128)(2,1)S(1)}, bf16[4,512]{1,0:T(4,128)(2,1)}, u32[]{:S(2)}) copy-start(bf16[4,512]{1,0:T(4,128)(2,1)} %param.20) | copy-start | bytes 12292
  6.6 8.1 %copy-start.24 = (f32[512]{0:T(512)S(1)}, f32[512]{0:T(512)}, u32[]{:S(2)}) copy-start(f32[512]{0:T(512)} %param.23) | copy-start | bytes 6148
  6.6 242.6 %all-gather.2.cloned.1.call-start = ((), (), s32[]{:S(2)}) async-start(), calls=%async_computation.4 | async-start | bytes 17842176 | tf_op jit(solution)/shard_map/all_gather | solution.py:14
  8.9 22.4 %collective-permute-start = (bf16[3,512]{1,0:T(4,128)(2,1)S(1)}, bf16[3,512]{1,0:T(4,128)(2,1)S(1)}, u32[]{:S(2)}, u32[]{:S(2)}) collective-permute-start(bf16[3,512]{1,0:T(4,128)(2,1)S(1)} %slice.393), channel_id=1, source_target_pairs={{0,4},{4,8},{8,12},{12,16},{16,20},{20,24},{24,28},{28,32},{32,36}... | collective-permute-start | bytes 9224 | tf_op jit(solution)/shard_map/ppermute | solution.py:27
  31.4 0.9 copy-start.26
  32.4 0.9 copy-start.27
  33.3 1.4 copy-start.10
  67.2 4.3 %copy-start.14 = (f32[176,512]{1,0:T(8,128)S(1)}, f32[176,512]{1,0:T(8,128)}, u32[]{:S(2)}) copy-start(f32[176,512]{1,0:T(8,128)} %slice.412) | copy-start | bytes 1081348
  67.2 4.3 %copy-start.15 = (f32[176,512]{1,0:T(8,128)S(1)}, f32[176,512]{1,0:T(8,128)}, u32[]{:S(2)}) copy-start(f32[176,512]{1,0:T(8,128)} %slice.411) | copy-start | bytes 1081348
  77.4 0.8 copy-start.23
  80.2 1.6 copy-start.11
  80.2 1.6 copy-start.12
  82.8 1.0 copy-start.13
  91.3 2.2 copy-start.2
  93.5 1.3 copy-start.3
  93.5 1.6 copy-start.6
  93.5 1.8 copy-start.7
  96.8 3.1 copy-start.8
  99.9 3.0 copy-start.5
  103.0 3.1 copy-start.4
  109.1 51.5 %copy-start.9 = (f32[704,512]{1,0:T(8,128)S(1)}, f32[704,512]{1,0:T(8,128)}, u32[]{:S(2)}) copy-start(f32[704,512]{1,0:T(8,128)} %pad.144) | copy-start | bytes 4325380
  111.4 26.0 %all-to-all-start = ((f32[32,2,512]{2,1,0:T(2,128)}), f32[32,2,512]{2,1,0:T(2,128)}, u32[]{:S(2)}, u32[]{:S(2)}) async-start(f32[32,2,512]{2,1,0:T(2,128)} %broadcast_in_dim.34), calls=%async_computation | async-start | bytes 262144 | tf_op jit(solution)/shard_map/all_to_all | solution.py:32
  166.7 37.8 %all-to-all-start.1 = ((bf16[4,176,2048]{2,1,0:T(8,128)(2,1)}), bf16[4,176,2048]{2,1,0:T(8,128)(2,1)S(1)}, u32[]{:S(2)}, u32[]{:S(2)}) async-start(bf16[4,176,2048]{2,1,0:T(8,128)(2,1)} %bitcast.53), calls=%async_computation.1 | async-start | bytes 5767168 | tf_op jit(solution)/shard_map/all_to_all | solution.py:81
  171.0 36.5 %copy-start.20 = (f32[2048]{0:T(1024)S(1)}, f32[2048]{0:T(1024)}, u32[]{:S(2)}) copy-start(f32[2048]{0:T(1024)} %param.26) | copy-start | bytes 24580
  206.1 3.2 copy-start.21
  211.6 4.9 %copy-start.18 = (bf16[3,1408]{1,0:T(4,128)(2,1)S(1)}, bf16[3,1408]{1,0:T(4,128)(2,1)}, u32[]{:S(2)}) copy-start(bf16[3,1408]{1,0:T(4,128)(2,1)} %param.31) | copy-start | bytes 25348
  211.6 4.9 %copy-start.19 = (bf16[3,1408]{1,0:T(4,128)(2,1)S(1)}, bf16[3,1408]{1,0:T(4,128)(2,1)}, u32[]{:S(2)}) copy-start(bf16[3,1408]{1,0:T(4,128)(2,1)} %param.32) | copy-start | bytes 25348
  211.6 37.6 %all-to-all-start.2 = ((bf16[4,176,2048]{2,1,0:T(8,128)(2,1)}), bf16[4,176,2048]{2,1,0:T(8,128)(2,1)}, u32[]{:S(2)}, u32[]{:S(2)}) async-start(bf16[4,176,2048]{2,1,0:T(8,128)(2,1)} %broadcast_in_dim.37), calls=%async_computation.2 | async-start | bytes 5767168 | tf_op jit(solution)/shard_map/all_to_all | solution.py:32
  249.2 8.4 %copy-start.25 = (bf16[2048,4224]{1,0:T(8,128)(2,1)S(1)}, bf16[2048,4224]{1,0:T(8,128)(2,1)}, u32[]{:S(2)}) copy-start(bf16[2048,4224]{1,0:T(8,128)(2,1)} %all-gather.2.cloned.1.call-done) | copy-start | bytes 51904516
  264.1 5.0 %collective-permute-start.1 = (bf16[2,2,1408]{2,1,0:T(2,128)(2,1)S(1)}, bf16[2,2,1408]{2,1,0:T(2,128)(2,1)S(1)}, u32[]{:S(2)}, u32[]{:S(2)}) collective-permute-start(bf16[2,2,1408]{2,1,0:T(2,128)(2,1)S(1)} %pad_maximum_fusion.15), channel_id=1, source_target_pairs={{0,4},{4,8},{8,12},{12,16},{16,20},{20,24},{24,28},{28,32},{32,36}... | collective-permute-start | bytes 33800 | tf_op jit(solution)/shard_map/ppermute | solution.py:27
  324.8 2.8 copy-start.22
  324.8 4.1 %copy-start.1 = (bf16[512,2048]{1,0:T(8,128)(2,1)S(1)}, bf16[512,2048]{1,0:T(8,128)(2,1)}, u32[]{:S(2)}) copy-start(bf16[512,2048]{1,0:T(8,128)(2,1)} %param.25) | copy-start | bytes 6291460
Sparse Core Ops, SparseCore 0:
  9.2 128.0 all-gather.1
where the time goes:
time: 338 us; the launch traced here: 336 us
  waiting for transfers between devices  101 us (30%)
  local copies, waits for them, and re-layouts  79.5 us (24%)
  blocking collectives  39.6 us (12%)
  other arithmetic  38.3 us (11%)
  matrix products  35.2 us (10%)
  starting transfers between devices  27.3 us (8%)
  between operations  14.4 us (4%)
    all_to_all x2, waiting for transfers between devices, copy_for_each(): return lax.all_to_all(copies, axis, split_axis=0, concat_axis=0, tiled=True)  50.6 us
    all_to_all x1, blocking collectives, summed_on_arrival(): lax.all_to_all(tiles, axis, split_axis=0, concat_axis=0, tiled=True)  39.6 us
    slice x64, local copies, waits for them, and re-layouts, local(): lax.associative_scan(linear_pair, (jnp.exp(log_decay), drive), axis=0)  35.4 us
    all_to_all x1, waiting for transfers between devices, summed_on_arrival(): lax.all_to_all(tiles, axis, split_axis=0, concat_axis=0, tiled=True)  33.6 us
    pad x32, local copies, waits for them, and re-layouts, local(): lax.associative_scan(linear_pair, (jnp.exp(log_decay), drive), axis=0)  20.6 us
    ppermute x2, waiting for transfers between devices, from_behind(): lax.ppermute(value, axis, [(source, source + steps) for source in range(i...  17 us
    slice x16, local copies, waits for them, and re-layouts, joined_by_halves(): part[side::2]  16.4 us
    dot_general x1, matrix products, local(): jnp.dot(chosen, down_whole, preferred_element_type=jnp.float32)  13.3 us
  transfers between devices with their start and end apart: 6, of which 5 were waited for; matrix products, arithmetic and copies ran while one was open for 34% of the time, Pallas kernels for 0%

commit v1 on v0

v1 whole, which is shorter than its diff:
```python
import functools

import jax
import jax.numpy as jnp
from jax import lax
from jax.experimental import pallas as pl
from jax.experimental.pallas import tpu as pltpu
from jax.sharding import PartitionSpec as P

EPS = 1e-06
GATE_SCALE = 8.0
LANES = 128
SEGMENTS = 8
TEAM = 8
SQRT_2_PI = 0.7978845608028654


def gelu(v):
    return 0.5 * v * (1.0 + jnp.tanh(SQRT_2_PI * (v + 0.044715 * (v * v * v))))


def sigmoid(v):
    return 1.0 / (1.0 + jnp.exp(-v))


def aligned(start, size, multiple):
    return pl.ds(pl.multiple_of(start, multiple), size)


def layer_kernel(
    num_sp,
    num_tp,
    mix_hbm,
    gate_hbm,
    jump_hbm,
    resid_hbm,
    outw_hbm,
    gw_hbm,
    vw_hbm,
    dw_hbm,
    mix_kernel,
    recur_map,
    input_map,
    coef,
    mix_gain,
    inner_gain,
    final_gain,
    gate_kernel,
    value_kernel,
    out_ref,
    wgv,
    wd,
    mixb,
    halo,
    gateb,
    a_s,
    b_s,
    gel,
    xpad,
    maps,
    branch,
    outw,
    resid,
    own_ab,
    team_ab,
    team_total,
    far_ab,
    rs1_send,
    rs1_recv,
    rs2_send,
    rs2_recv,
    mixed,
    hidden,
    normed,
    up,
    act,
    load_sem,
    wload_sem,
    halo_sem,
    tail_sem,
    team_send,
    team_recv,
    far_send,
    far_recv,
    ring_send,
    ring_recv,
    twin_send,
    twin_recv,
    rs1_ssem,
    rs1_rsem,
    rs2_ssem,
    rs2_rsem,
    ag_ssem,
    ag_rsem,
):
    sp = lax.axis_index("sp")
    t = lax.axis_index("tp")
    length, channels = mixb.shape
    groups = channels // LANES
    shard = gw_hbm.shape[0]
    width = gw_hbm.shape[1]
    tiles = width // LANES
    model = outw.shape[1]
    rows = length // num_tp
    half = model // 2
    sub = half // 2
    chips = num_sp // 2
    far = chips // 2
    core = lax.rem(sp, 2)
    chip = sp // 2
    twin = sp + 1 - 2 * core
    after = lax.rem(sp + 1, num_sp)
    before = lax.rem(sp + num_sp - 1, num_sp)
    z_next = (lax.rem(sp + 2, num_sp), lax.rem(sp + num_sp - 2, num_sp))
    t_next = (lax.rem(t + 1, num_tp), lax.rem(t + num_tp - 1, num_tp))
    place = lax.rem(sp, TEAM)
    team = sp // TEAM
    teams = num_sp // TEAM

    def sp_id(index):
        return {"sp": index}

    def tp_id(index):
        return {"tp": index}

    def mate(k):
        return team * TEAM + lax.rem(place + k, TEAM)

    def far_mate(k):
        return lax.rem(sp + TEAM * k, num_sp)

    barrier = pltpu.get_barrier_semaphore()
    partners = [sp_id(after), sp_id(before), sp_id(z_next[0]), sp_id(z_next[1])]
    partners += [sp_id(mate(k)) for k in range(1, TEAM)]
    partners += [sp_id(far_mate(k)) for k in range(1, teams)]
    partners += [tp_id(lax.rem(t + k, num_tp)) for k in range(1, num_tp)]
    for partner in partners:
        pl.semaphore_signal(barrier, inc=1, device_id=partner, device_id_type=pl.DeviceIdType.MESH)

    own_rows = aligned(sp * shard, shard, shard)

    def weight_loads():
        copies = []
        for j in range(tiles):
            for side, source in enumerate((gw_hbm, vw_hbm)):
                copies.append(
                    pltpu.make_async_copy(
                        source.at[:, pl.ds(j * LANES, LANES)],
                        wgv.at[own_rows, pl.ds((2 * j + side) * LANES, LANES)],
                        wload_sem.at[2 * j + side],
                    )
                )
        copies.append(pltpu.make_async_copy(dw_hbm, wd.at[own_rows, :], wload_sem.at[2 * tiles]))
        return copies

    mix_load = pltpu.make_async_copy(mix_hbm, mixb, load_sem.at[0])
    jump_loads = [
        pltpu.make_async_copy(
            jump_hbm.at[:, pl.ds(g * LANES, LANES)], a_s.at[g], load_sem.at[5 + g]
        )
        for g in range(groups)
    ]
    gate_load = pltpu.make_async_copy(gate_hbm, gateb, load_sem.at[1])
    outw_load = pltpu.make_async_copy(outw_hbm, outw, load_sem.at[2])
    resid_load = pltpu.make_async_copy(
        resid_hbm.at[aligned(t * rows, rows, 16), :], resid, load_sem.at[3]
    )
    mix_load.start()
    loads = weight_loads()
    for copy in loads:
        copy.start()
    for copy in jump_loads:
        copy.start()
    gate_load.start()
    outw_load.start()
    resid_load.start()
    for g in range(groups):
        maps[g, :, :LANES] = recur_map[g]
        maps[g, :, LANES:] = input_map[g]

    pl.semaphore_wait(barrier, len(partners))

    halo_copy = pltpu.make_async_remote_copy(
        src_ref=mix_hbm.at[pl.ds(length - 16, 16), :],
        dst_ref=halo,
        send_sem=halo_sem.at[0],
        recv_sem=halo_sem.at[1],
        device_id=sp_id(after),
        device_id_type=pl.DeviceIdType.MESH,
    )
    halo_copy.start()
    for copy in loads:
        copy.wait()

    near = 2 * (far - 1)
    gv_steps = near + 1
    d_steps = far
    steps = gv_steps + d_steps

    def piece(way, index):
        if index < gv_steps:
            distance, part = index // 2 + 1, index % 2
            if index == near:
                part = way
        else:
            distance, part = index - gv_steps + 1, None
        origin = lax.rem(chip + (chips - distance if way == 0 else distance), chips)
        return distance, part, origin

    def piece_ref(origin, part, way, distance):
        start = (2 * origin + core) * shard
        if part is not None:
            return wgv.at[aligned(start, shard, shard), pl.ds(part * width, width)]
        if distance == far:
            share = shard // 2
            return wd.at[aligned(start + way * share, share, share), :]
        return wd.at[aligned(start, shard, shard), :]

    def ring_copy(way, index):
        distance, part, _ = piece(way, index)
        source = distance - 1
        origin = lax.rem(chip + (chips - source if way == 0 else source), chips)
        ref = piece_ref(origin, part, way, distance)
        return pltpu.make_async_remote_copy(
            src_ref=ref,
            dst_ref=ref,
            send_sem=ring_send.at[way, index],
            recv_sem=ring_recv.at[way, index],
            device_id=sp_id(z_next[way]),
            device_id_type=pl.DeviceIdType.MESH,
        )

    def twin_copy(ref, kind):
        return pltpu.make_async_remote_copy(
            src_ref=ref,
            dst_ref=ref,
            send_sem=twin_send.at[kind],
            recv_sem=twin_recv.at[kind],
            device_id=sp_id(twin),
            device_id_type=pl.DeviceIdType.MESH,
        )

    def arrived(way, index):
        distance, part, origin = piece(way, index)
        ref = piece_ref(origin, part, way, distance)
        pltpu.make_async_remote_copy(
            src_ref=ref,
            dst_ref=ref,
            send_sem=ring_send.at[way, index],
            recv_sem=ring_recv.at[way, index],
            device_id=sp_id(z_next[way]),
            device_id_type=pl.DeviceIdType.MESH,
        ).wait_recv()
        if index < gv_steps:
            onward = index + 2
            if distance < far and (distance < far - 1 or part == way):
                onward = near if distance == far - 1 else onward
                ring_copy(way, onward).start()
        elif distance < far:
            ring_copy(way, index + 1).start()
        twin_copy(ref, 0 if index < gv_steps else 1).start()

    progress = [0]

    def pump(count):
        for _ in range(count):
            index = progress[0]
            if index >= steps:
                return
            if index == gv_steps - 2:
                for way in range(2):
                    ring_copy(way, gv_steps).start()
                twin_copy(piece_ref(chip, None, 0, 0), 1).start()
            for way in range(2):
                arrived(way, index)
            progress[0] = index + 1

    for index in range(2):
        for way in range(2):
            ring_copy(way, index).start()
    twin_copy(wgv.at[own_rows, :], 0).start()

    mix_load.wait()
    for g in range(groups):
        jump_loads[g].wait()
    xpad[pl.ds(8, length), :] = mixb[...].astype(jnp.float32)
    halo_copy.wait_recv()
    edge = halo[...].astype(jnp.float32)[8:, :]
    xpad[pl.ds(0, 8), :] = jnp.where(sp > 0, edge, 0.0)
    taps = mix_kernel[...].astype(jnp.float32)
    chunk = 64

    def gates(i):
        for g in range(groups):
            lanes = slice(g * LANES, (g + 1) * LANES)
            window = xpad[aligned(i * chunk, chunk + 8, 8), lanes]
            total = window[8:] * taps[3:4, lanes]
            for back in range(1, 4):
                total += pltpu.roll(window, back, 0)[8:] * taps[3 - back : 4 - back, lanes]
            conv = total.astype(jnp.bfloat16)
            both = jnp.dot(conv, maps[g], preferred_element_type=jnp.float32)
            at = aligned(i * chunk, chunk, 8)
            log_decay = sigmoid(both[:, :LANES]) * coef[:, lanes] + a_s[g, at, :]
            decay = jnp.exp(log_decay)
            loss = -jnp.tanh(log_decay) * (decay * decay + 1.0)
            drive = jnp.sqrt(loss) * sigmoid(both[:, LANES:]) * conv.astype(jnp.float32)
            a_s[g, at, :] = decay
            b_s[g, at, :] = drive

    pl.loop(0, length // chunk)(gates)
    pump(1)

    stretch = length // SEGMENTS

    def scan_step(i, carry):
        result = []
        for g in range(groups):
            product, state = carry[g]
            at = pl.ds(i, SEGMENTS, stride=stretch)
            decay = a_s[g, at, :]
            state = decay * state + b_s[g, at, :]
            product = product * decay
            a_s[g, at, :] = product
            b_s[g, at, :] = state
            result.append((product, state))
        return tuple(result)

    unit = jnp.ones((SEGMENTS, LANES), jnp.float32)
    ends = lax.fori_loop(0, stretch, scan_step, tuple((unit, unit * 0.0) for _ in range(groups)))
    segments = []
    for g in range(groups):
        product, state = ends[g]
        passed, held = unit[:1], unit[:1] * 0.0
        firsts, seconds = [], []
        for s in range(SEGMENTS):
            firsts.append(passed)
            seconds.append(held)
            held = product[s : s + 1] * held + state[s : s + 1]
            passed = passed * product[s : s + 1]
        segments.append((jnp.concatenate(firsts, axis=0), jnp.concatenate(seconds, axis=0)))
        own_ab[0:1, pl.ds(g * LANES, LANES)] = passed
        own_ab[1:2, pl.ds(g * LANES, LANES)] = held

    def team_copy(k):
        return pltpu.make_async_remote_copy(
            src_ref=own_ab,
            dst_ref=team_ab.at[TEAM - 1 - k],
            send_sem=team_send.at[k - 1],
            recv_sem=team_recv.at[k - 1],
            device_id=sp_id(mate(k)),
            device_id_type=pl.DeviceIdType.MESH,
        )

    def far_copy(k):
        return pltpu.make_async_remote_copy(
            src_ref=team_total,
            dst_ref=far_ab.at[k - 1],
            send_sem=far_send.at[k - 1],
            recv_sem=far_recv.at[k - 1],
            device_id=sp_id(far_mate(k)),
            device_id_type=pl.DeviceIdType.MESH,
        )

    for k in range(1, TEAM):
        team_copy(k).start()

    gate_load.wait()
    chunk2 = 176

    def gate_values(i):
        at = aligned(i * chunk2, chunk2, 16)
        for g in range(groups):
            gel[g, at, :] = gelu(gateb[at, g * LANES : (g + 1) * LANES].astype(jnp.float32))

    pl.loop(0, length // chunk2)(gate_values)

    for k in range(1, TEAM):
        team_copy(k).wait_recv()
    own = own_ab[...]
    head_a, head_b = jnp.ones_like(own[0:1]), jnp.zeros_like(own[0:1])
    tail_a, tail_b = own[0:1], own[1:2]
    for k in range(TEAM - 1, 0, -1):
        pair = team_ab[TEAM - 1 - k]
        inside = k <= place
        head_b = jnp.where(inside, pair[0:1] * head_b + pair[1:2], head_b)
        head_a = jnp.where(inside, pair[0:1] * head_a, head_a)
    for k in range(TEAM - 1, 0, -1):
        pair = team_ab[TEAM - 1 - k]
        behind = k > place
        tail_b = jnp.where(behind, pair[0:1] * tail_b + pair[1:2], tail_b)
        tail_a = jnp.where(behind, pair[0:1] * tail_a, tail_a)
    team_total[0:1, :] = head_a * tail_a
    team_total[1:2, :] = tail_a * head_b + tail_b
    for k in range(1, teams):
        far_copy(k).start()
    pump(2)
    for k in range(1, teams):
        far_copy(k).wait_recv()
    carried = jnp.zeros_like(own[0:1])
    for k in range(teams - 1, 0, -1):
        pair = far_ab[k - 1]
        carried = jnp.where(k <= team, pair[0:1] * carried + pair[1:2], carried)
    carried = head_a * carried + head_b

    inflow = [
        segments[g][0] * carried[:, g * LANES : (g + 1) * LANES] + segments[g][1]
        for g in range(groups)
    ]

    def finish_step(i):
        for g in range(groups):
            at = pl.ds(i, SEGMENTS, stride=stretch)
            state = a_s[g, at, :] * inflow[g] + b_s[g, at, :]
            b_s[g, at, :] = state * gel[g, at, :]

    pl.loop(0, stretch)(finish_step)
    for g in range(groups):
        branch[:, pl.ds(g * LANES, LANES)] = b_s[g].astype(jnp.bfloat16)
    outw_load.wait()
    pump(1)

    def reduce_scatter(partial, send, recv, ssem, rsem, finish, pumps):
        copies = []
        for s in range(num_tp):
            for q in range(2):
                for way in range(2):
                    shift = num_tp - 1 - s if way == 0 else 1 + s
                    block = lax.rem(t + shift, num_tp)
                    column = way * half + q * sub
                    value = partial(block, column)
                    if s > 0:
                        copies[4 * (s - 1) + 2 * q + way].wait_recv()
                        value = value + recv[way, s - 1, q].astype(jnp.float32)
                    if s < num_tp - 1:
                        send[way, s, q] = value.astype(jnp.bfloat16)
                        copy = pltpu.make_async_remote_copy(
                            src_ref=send.at[way, s, q],
                            dst_ref=recv.at[way, s, q],
                            send_sem=ssem.at[way, s, q],
                            recv_sem=rsem.at[way, s, q],
                            device_id=tp_id(t_next[way]),
                            device_id_type=pl.DeviceIdType.MESH,
                        )
                        copy.start()
                        copies.append(copy)
                    else:
                        finish(column, value)
                pump(pumps)
        return copies

    def mix_partial(block, column):
        return jnp.dot(
            branch[aligned(block * rows, rows, 16), :],
            outw[:, pl.ds(column, sub)],
            preferred_element_type=jnp.float32,
        )

    def keep_mixed(column, value):
        mixed[:, pl.ds(column, sub)] = value.astype(jnp.bfloat16)

    rs1_copies = reduce_scatter(
        mix_partial, rs1_send, rs1_recv, rs1_ssem, rs1_rsem, keep_mixed, 1
    )
    resid_load.wait()

    def scaled(value, gain):
        mean = jnp.mean(value * value, axis=-1, keepdims=True)
        return value * lax.rsqrt(mean + EPS) * gain[...]

    def norm_rows(i):
        at = aligned(i * 16, 16, 16)
        stream = resid[at, :].astype(jnp.float32)
        stream += scaled(mixed[at, :].astype(jnp.float32), mix_gain)
        stream = stream.astype(jnp.bfloat16)
        hidden[at, :] = stream
        normed[aligned(t * rows + i * 16, 16, 16), :] = scaled(
            stream.astype(jnp.float32), inner_gain
        ).astype(jnp.bfloat16)

    pl.loop(0, rows // 16)(norm_rows)

    order = ((0, 1, 2, 3), (2, 3, 0, 1))

    def gather_copy(way, index):
        source = 0 if index < 4 else 1
        block = lax.rem(t + (num_tp - source if way == 0 else source), num_tp)
        column = order[way][index % 4] * sub
        ref = normed.at[aligned(block * rows, rows, 16), pl.ds(column, sub)]
        return pltpu.make_async_remote_copy(
            src_ref=ref,
            dst_ref=ref,
            send_sem=ag_ssem.at[way, index],
            recv_sem=ag_rsem.at[way, index],
            device_id=tp_id(t_next[way]),
            device_id_type=pl.DeviceIdType.MESH,
        )

    def gather_wait(way, index):
        source = 1 if index < 4 else 2
        block = lax.rem(t + (num_tp - source if way == 0 else source), num_tp)
        column = order[way][index % 4] * sub
        ref = normed.at[aligned(block * rows, rows, 16), pl.ds(column, sub)]
        pltpu.make_async_remote_copy(
            src_ref=ref,
            dst_ref=ref,
            send_sem=ag_ssem.at[way, index],
            recv_sem=ag_rsem.at[way, index],
            device_id=tp_id(t_next[way]),
            device_id_type=pl.DeviceIdType.MESH,
        ).wait_recv()

    for index in range(4):
        for way in range(2):
            gather_copy(way, index).start()
    for index in range(2):
        for way in range(2):
            gather_wait(way, index)
            gather_copy(way, index + 4).start()
        pump(1)

    tail_copy = pltpu.make_async_remote_copy(
        src_ref=up.at[pl.ds(length, 16), :],
        dst_ref=up.at[pl.ds(0, 16), :],
        send_sem=tail_sem.at[0],
        recv_sem=tail_sem.at[1],
        device_id=sp_id(after),
        device_id_type=pl.DeviceIdType.MESH,
    )

    def up_block(block):
        source = aligned(block * rows, rows, 16)
        target = aligned(16 + block * rows, rows, 16)

        def tile(j):
            columns = aligned(j * 2 * LANES, 2 * LANES, LANES)
            up[target, columns] = jnp.dot(
                normed[source, :], wgv[:, columns], preferred_element_type=jnp.float32
            ).astype(jnp.bfloat16)

        pl.loop(0, tiles)(tile)

        @pl.when(block == num_tp - 1)
        def _():
            tail_copy.start()

    def act_block(block):
        @pl.when(block == 0)
        def _():
            tail_copy.wait_recv()

            @pl.when(sp == 0)
            def _():
                up[pl.ds(0, 16), :] = jnp.zeros((16, 2 * width), jnp.bfloat16)

        window = aligned(block * rows, rows + 16, 16)
        target = aligned(block * rows, rows, 16)

        def tile(j):
            columns = aligned(j * LANES, LANES, LANES)
            results = []
            for side, kernel in enumerate((gate_kernel, value_kernel)):
                start = (2 * j + side) * LANES
                value = up[window, aligned(start, LANES, LANES)].astype(jnp.float32)
                tap = kernel[:, columns].astype(jnp.float32)
                total = value[16:] * tap[2:3]
                for back in range(1, 3):
                    total += pltpu.roll(value, back, 0)[16:] * tap[2 - back : 3 - back]
                results.append(total)
            act[target, columns] = (gelu(results[0]) * results[1]).astype(jnp.bfloat16)

        pl.loop(0, tiles)(tile)

    def around(k):
        return lax.rem(t + k, num_tp)

    pump(gv_steps - progress[0])
    rival = wgv.at[pl.ds(0, chips * shard), :]
    pltpu.make_async_copy(rival, rival, twin_recv.at[0]).wait()
    up_block(around(0))
    pump(1)
    for index in range(2, 4):
        gather_wait(0, index)
    up_block(around(num_tp - 1))
    pump(1)
    for index in range(2, 4):
        gather_wait(1, index)
    up_block(around(1))
    pump(1)
    act_block(around(0))
    pump(1)
    act_block(around(1))
    pump(1)
    for index in range(4, 6):
        for way in range(2):
            gather_wait(way, index)
    up_block(around(2))
    pump(1)
    act_block(around(2))
    pump(1)
    act_block(around(num_tp - 1))
    pump(steps)
    rival = wd.at[pl.ds(0, chips * shard), :]
    pltpu.make_async_copy(rival, rival, twin_recv.at[1]).wait()

    def down_partial(block, column):
        return lax.dot_general(
            act[aligned(block * rows, rows, 16), :],
            wd[pl.ds(column, sub), :],
            (((1,), (1,)), ((), ())),
            preferred_element_type=jnp.float32,
        )

    rs2_copies = reduce_scatter(
        down_partial, rs2_send, rs2_recv, rs2_ssem, rs2_rsem, keep_mixed, 0
    )

    def last_rows(i):
        at = aligned(i * 16, 16, 16)
        stream = hidden[at, :].astype(jnp.float32)
        stream += scaled(mixed[at, :].astype(jnp.float32), final_gain)
        out_ref[at, :] = stream.astype(jnp.bfloat16)

    pl.loop(0, rows // 16)(last_rows)

    halo_copy.wait_send()
    tail_copy.wait_send()
    for k in range(1, TEAM):
        team_copy(k).wait_send()
    for k in range(1, teams):
        far_copy(k).wait_send()
    for index in range(steps):
        for way in range(2):
            ring_copy(way, index).wait_send()
    gathered = wgv.at[pl.ds(0, chips * shard), :]
    pltpu.make_async_copy(gathered, gathered, twin_send.at[0]).wait()
    gathered = wd.at[pl.ds(0, chips * shard), :]
    pltpu.make_async_copy(gathered, gathered, twin_send.at[1]).wait()
    for copy in rs1_copies + rs2_copies:
        copy.wait_send()
    for index in range(6):
        for way in range(2):
            gather_copy(way, index).wait_send()


def local(
    num_sp,
    num_tp,
    residual,
    mix_input,
    gate_input,
    mix_kernel,
    recur_gate_map,
    input_gate_map,
    decay_param,
    jump_log,
    out_weight,
    mix_gain,
    inner_gain,
    final_gain,
    gate_weight,
    value_weight,
    gate_kernel,
    value_kernel,
    down_weight,
):
    length, channels = mix_input.shape
    model = residual.shape[1]
    shard, width = gate_weight.shape
    rows = length // num_tp
    sub = model // 4
    groups = channels // LANES
    coef = (-GATE_SCALE * jax.nn.softplus(-decay_param)).reshape(1, channels)
    far = num_sp // 4
    steps = 2 * (far - 1) + 1 + far
    hbm = pl.BlockSpec(memory_space=pl.ANY)
    vmem = pl.BlockSpec(memory_space=pltpu.VMEM)
    bf16, f32 = jnp.bfloat16, jnp.float32
    dma = pltpu.SemaphoreType.DMA
    flow = (2, num_tp - 1, 2, rows, sub)
    return pl.pallas_call(
        functools.partial(layer_kernel, num_sp, num_tp),
        out_shape=jax.ShapeDtypeStruct((rows, model), bf16),
        in_specs=[hbm] * 8 + [vmem] * 9,
        out_specs=vmem,
        scratch_shapes=[
            pltpu.VMEM((num_sp * shard, 2 * width), bf16),
            pltpu.VMEM((num_sp * shard, width), bf16),
            pltpu.VMEM((length, channels), bf16),
            pltpu.VMEM((16, channels), bf16),
            pltpu.VMEM((length, channels), bf16),
            pltpu.VMEM((groups, length, LANES), f32),
            pltpu.VMEM((groups, length, LANES), f32),
            pltpu.VMEM((groups, length, LANES), f32),
            pltpu.VMEM((length + 8, channels), f32),
            pltpu.VMEM((groups, LANES, 2 * LANES), bf16),
            pltpu.VMEM((length, channels), bf16),
            pltpu.VMEM((channels, model), bf16),
            pltpu.VMEM((rows, model), bf16),
            pltpu.VMEM((2, channels), f32),
            pltpu.VMEM((TEAM - 1, 2, channels), f32),
            pltpu.VMEM((2, channels), f32),
            pltpu.VMEM((num_sp // TEAM - 1, 2, channels), f32),
            pltpu.VMEM(flow, bf16),
            pltpu.VMEM(flow, bf16),
            pltpu.VMEM(flow, bf16),
            pltpu.VMEM(flow, bf16),
            pltpu.VMEM((rows, model), bf16),
            pltpu.VMEM((rows, model), bf16),
            pltpu.VMEM((length, model), bf16),
            pltpu.VMEM((16 + length, 2 * width), bf16),
            pltpu.VMEM((length, width), bf16),
            dma((5 + groups,)),
            dma((2 * (width // LANES) + 1,)),
            dma((2,)),
            dma((2,)),
            dma((TEAM - 1,)),
            dma((TEAM - 1,)),
            dma((num_sp // TEAM - 1,)),
            dma((num_sp // TEAM - 1,)),
            dma((2, steps)),
            dma((2, steps)),
            dma((2,)),
            dma((2,)),
            dma(flow[:3]),
            dma(flow[:3]),
            dma(flow[:3]),
            dma(flow[:3]),
            dma((2, 6)),
            dma((2, 6)),
        ],
        compiler_params=pltpu.CompilerParams(
            collective_id=0, has_side_effects=True, vmem_limit_bytes=67043328
        ),
    )(
        mix_input,
        gate_input,
        jump_log,
        residual,
        out_weight,
        gate_weight,
        value_weight,
        down_weight.T,
        mix_kernel,
        recur_gate_map,
        input_gate_map,
        coef,
        mix_gain.reshape(1, model),
        inner_gain.reshape(1, model),
        final_gain.reshape(1, model),
        gate_kernel,
        value_kernel,
    )


def solution(mesh):
    return jax.shard_map(
        functools.partial(local, mesh.shape["sp"], mesh.shape["tp"]),
        mesh=mesh,
        in_specs=(
            P(("grp", "sp"), None),
            P(("grp", "sp"), "tp"),
            P(("grp", "sp"), "tp"),
            P(None, "tp"),
            P("tp", None, None),
            P("tp", None, None),
            P("tp"),
            P(("grp", "sp"), "tp"),
            P("tp", None),
            P(),
            P(),
            P(),
            P("sp", "tp"),
            P("sp", "tp"),
            P(None, "tp"),
            P(None, "tp"),
            P("tp", "sp"),
        ),
        out_specs=P(("grp", "sp", "tp"), None),
        check_vma=False,
    )
```

time: 338 us -> 180 us (0.53)
  Pallas kernels: 0 us -> 177 us
  waiting for transfers between devices: 101 us -> 0 us
  local copies, waits for them, and re-layouts: 79.5 us -> 2.04 us
  blocking collectives: 39.6 us -> 0 us
  other arithmetic: 38.3 us -> 1.28 us
  matrix products: 35.2 us -> 0 us
  starting transfers between devices: 27.3 us -> 0 us
  between operations: 14.4 us -> 0.01 us
    pallas_call x0 -> x1, Pallas kernels: none -> 177 us  [local(): pl.pallas_call(functools.partial(layer_kernel, num_sp, num_tp), out_shape...]
    all_to_all x3 -> x0, waiting for transfers between devices: 84.2 us -> none  [the longest x2 50.6 us: copy_for_each(): return lax.all_to_all(copies, axis, split_axis=0, concat_axis=0, tiled=True)]
    slice x84 -> x0, local copies, waits for them, and re-layouts: 52.9 us -> none  [the longest x64 35.4 us: local(): lax.associative_scan(linear_pair, (jnp.exp(log_decay), drive), axis=0)]
    all_to_all x1 -> x0, blocking collectives: 39.6 us -> none  [summed_on_arrival(): lax.all_to_all(tiles, axis, split_axis=0, concat_axis=0, tiled=True)]
    dot_general x6 -> x0, matrix products: 35.2 us -> none  [the longest x1 13.3 us: local(): jnp.dot(chosen, down_whole, preferred_element_type=jnp.float32)]
    pad x32 -> x0, local copies, waits for them, and re-layouts: 20.6 us -> none  [local(): lax.associative_scan(linear_pair, (jnp.exp(log_decay), drive), axis=0)]
    all_to_all x3 -> x0, starting transfers between devices: 17.2 us -> none  [the longest x2 12.9 us: copy_for_each(): return lax.all_to_all(copies, axis, split_axis=0, concat_axis=0, tiled=True)]
    ppermute x2 -> x0, waiting for transfers between devices: 17 us -> none  [from_behind(): lax.ppermute(value, axis, [(source, source + steps) for source in range(i...]
  transfers between devices with their start and end apart: 6 -> 0, of which waited for: 5 -> 0; matrix products, arithmetic and copies ran while one was open for 34% -> 0% of each run, Pallas kernels for 0% -> 0%
where the time goes in v1:
time: 180 us
  Pallas kernels  177 us (98%)
  local copies, waits for them, and re-layouts  2.04 us (1%)
    pallas_call x1, Pallas kernels, local(): pl.pallas_call(functools.partial(layer_kernel, num_sp, num_tp), out_shape...  177 us

profile of v1, /device:TPU:33, one launch (start us, length us, event | category | flops | bytes accessed | tf_op | source)
XLA Modules:
  0.0 179.9 jit_solution(9215521537391036655)
XLA Ops:
  0.0 1.3 fusion
  1.3 176.5 %shard_map.163 = bf16[176,2048]{1,0:T(8,128)(2,1)} custom-call(bf16[704,512]{1,0:T(8,128)(2,1)} %mix_hbm.1, bf16[704,512]{1,0:T(8,128)(2,1)} %gate_hbm.1, f32[704,512]{1,0:T(8,128)} %jump_hbm.1, bf16[704,2048]{1,0:T(8,128)(2,1)} %resid_hbm.1, bf16[512,2048]{1,0:T(8,128)(2,1)} %outw_hbm.1, bf16[64,1408]{1,0:T(8,128)(2,1)} %gw_hbm.1, bf16[64,1408]{1,0:T(8,128)(2,1)} %vw_hbm.1, ...), custom_call_target="tpu_custom_call" | custom-call | tf_op jit(solution)/shard_map/pallas_call | solution.py:680
  177.8 2.0 %copy.19 = bf16[176,2048]{1,0:T(8,128)(2,1)} copy(bf16[176,2048]{1,0:T(8,128)(2,1)} %shard_map.163) | data formatting | bytes 1441792

commit v2 on v1

--- a/solution.py
+++ b/solution.py
@@ -21,6 +21,16 @@
 
 def sigmoid(v):
     return 1.0 / (1.0 + jnp.exp(-v))
+
+
+def softplus(v):
+    z = jnp.exp(-jnp.abs(v))
+    ratio = z / (2.0 + z)
+    square = ratio * ratio
+    series = jnp.full_like(square, 1.0 / 19.0)
+    for power in range(17, 0, -2):
+        series = series * square + 1.0 / power
+    return jnp.maximum(v, 0.0) + 2.0 * ratio * series
 
 
 def aligned(start, size, multiple):
@@ -41,7 +51,7 @@
     mix_kernel,
     recur_map,
     input_map,
-    coef,
+    decay_param,
     mix_gain,
     inner_gain,
     final_gain,
@@ -84,6 +94,8 @@
     far_recv,
     ring_send,
     ring_recv,
+    pair_send,
+    pair_recv,
     twin_send,
     twin_recv,
     rs1_ssem,
@@ -94,6 +106,9 @@
     ag_rsem,
 ):
     sp = lax.axis_index("sp")
+    grp = lax.axis_index("grp")
+    parity = lax.rem(grp, 2)
+    pair_grp = grp + 1 - 2 * parity
     t = lax.axis_index("tp")
     length, channels = mixb.shape
     groups = channels // LANES
@@ -134,6 +149,7 @@
     partners += [sp_id(mate(k)) for k in range(1, TEAM)]
     partners += [sp_id(far_mate(k)) for k in range(1, teams)]
     partners += [tp_id(lax.rem(t + k, num_tp)) for k in range(1, num_tp)]
+    partners += [{"grp": pair_grp}]
     for partner in partners:
         pl.semaphore_signal(barrier, inc=1, device_id=partner, device_id_type=pl.DeviceIdType.MESH)
 
@@ -178,116 +194,105 @@
         maps[g, :, :LANES] = recur_map[g]
         maps[g, :, LANES:] = input_map[g]
 
-    pl.semaphore_wait(barrier, len(partners))
-
-    halo_copy = pltpu.make_async_remote_copy(
-        src_ref=mix_hbm.at[pl.ds(length - 16, 16), :],
-        dst_ref=halo,
-        send_sem=halo_sem.at[0],
-        recv_sem=halo_sem.at[1],
-        device_id=sp_id(after),
-        device_id_type=pl.DeviceIdType.MESH,
-    )
-    halo_copy.start()
-    for copy in loads:
-        copy.wait()
-
+    whole = (wgv, wd)
+    lone = ((2 * tiles // 3) * LANES, ((tiles + 1) // 3) * LANES)
     near = 2 * (far - 1)
-    gv_steps = near + 1
-    d_steps = far
-    steps = gv_steps + d_steps
-
-    def piece(way, index):
-        if index < gv_steps:
-            distance, part = index // 2 + 1, index % 2
-            if index == near:
-                part = way
-        else:
-            distance, part = index - gv_steps + 1, None
-        origin = lax.rem(chip + (chips - distance if way == 0 else distance), chips)
-        return distance, part, origin
-
-    def piece_ref(origin, part, way, distance):
-        start = (2 * origin + core) * shard
-        if part is not None:
-            return wgv.at[aligned(start, shard, shard), pl.ds(part * width, width)]
-        if distance == far:
-            share = shard // 2
-            return wd.at[aligned(start + way * share, share, share), :]
-        return wd.at[aligned(start, shard, shard), :]
-
-    def ring_copy(way, index):
-        distance, part, _ = piece(way, index)
-        source = distance - 1
-        origin = lax.rem(chip + (chips - source if way == 0 else source), chips)
-        ref = piece_ref(origin, part, way, distance)
+    per_stage = near + 1
+
+    def part_ref(stage, origin, part, side):
+        ref, size = whole[stage], lone[stage]
+        at = aligned((2 * origin + core) * shard, shard, shard)
+        if part == 0:
+            return ref.at[at, aligned(side * size, size, LANES)]
+        return ref.at[at, pl.ds(2 * size, ref.shape[1] - 2 * size)]
+
+    def origin_at(way, distance):
+        return lax.rem(chip + (chips - distance if way == 0 else distance), chips)
+
+    def what(way, index):
+        return index // 2 + 1, (way if index == near else index % 2)
+
+    def remote(ref, send_sem, recv_sem, device_id):
         return pltpu.make_async_remote_copy(
             src_ref=ref,
             dst_ref=ref,
-            send_sem=ring_send.at[way, index],
-            recv_sem=ring_recv.at[way, index],
-            device_id=sp_id(z_next[way]),
+            send_sem=send_sem,
+            recv_sem=recv_sem,
+            device_id=device_id,
             device_id_type=pl.DeviceIdType.MESH,
         )
 
-    def twin_copy(ref, kind):
-        return pltpu.make_async_remote_copy(
-            src_ref=ref,
-            dst_ref=ref,
-            send_sem=twin_send.at[kind],
-            recv_sem=twin_recv.at[kind],
-            device_id=sp_id(twin),
-            device_id_type=pl.DeviceIdType.MESH,
+    def ring_copy(way, stage, index, received=False):
+        distance, part = what(way, index)
+        ref = part_ref(stage, origin_at(way, distance - (0 if received else 1)), part, parity)
+        slot = stage * per_stage + index
+        return remote(
+            ref, ring_send.at[way, slot], ring_recv.at[way, slot], sp_id(z_next[way])
         )
 
-    def arrived(way, index):
-        distance, part, origin = piece(way, index)
-        ref = piece_ref(origin, part, way, distance)
-        pltpu.make_async_remote_copy(
-            src_ref=ref,
-            dst_ref=ref,
-            send_sem=ring_send.at[way, index],
-            recv_sem=ring_recv.at[way, index],
-            device_id=sp_id(z_next[way]),
-            device_id_type=pl.DeviceIdType.MESH,
-        ).wait_recv()
-        if index < gv_steps:
-            onward = index + 2
-            if distance < far and (distance < far - 1 or part == way):
-                onward = near if distance == far - 1 else onward
-                ring_copy(way, onward).start()
-        elif distance < far:
-            ring_copy(way, index + 1).start()
-        twin_copy(ref, 0 if index < gv_steps else 1).start()
-
+    def pair_copy(way, stage, distance, received=False):
+        side = 1 - parity if received else parity
+        ref = part_ref(stage, origin_at(way, distance), 0, side)
+        slot = stage * per_stage + way * far + distance - 1
+        return remote(ref, pair_send.at[slot], pair_recv.at[slot], {"grp": pair_grp})
+
+    def twin_copy(ref, stage):
+        return remote(ref, twin_send.at[stage], twin_recv.at[stage], sp_id(twin))
+
+    def arrived(way, stage, index):
+        distance, part = what(way, index)
+        ring_copy(way, stage, index, True).wait_recv()
+        if distance < far - 1:
+            ring_copy(way, stage, index + 2).start()
+        elif distance == far - 1 and part == way:
+            ring_copy(way, stage, near).start()
+        if part == 0:
+            pair_copy(way, stage, distance).start()
+        twin_copy(part_ref(stage, origin_at(way, distance), part, parity), stage).start()
+
+    def crossed(way, stage, distance):
+        pair_copy(way, stage, distance, True).wait_recv()
+        twin_copy(part_ref(stage, origin_at(way, distance), 0, 1 - parity), stage).start()
+
+    def ring_start(stage, part):
+        for way in range(2):
+            ring_copy(way, stage, part).start()
+
+    def event(stage, index):
+        if index < per_stage:
+            for way in range(2):
+                arrived(way, stage, index)
+            if index % 2 == 1 and index > 1:
+                for way in range(2):
+                    crossed(way, stage, (index - 1) // 2)
+        else:
+            for way in range(2):
+                crossed(way, stage, far - 1)
+            crossed(0, stage, far)
+
+    events = [(0, k) for k in range(per_stage)] + [(1, 0), (0, per_stage)]
+    first_done = len(events)
+    events += [(1, k) for k in range(1, per_stage + 1)]
     progress = [0]
 
     def pump(count):
         for _ in range(count):
-            index = progress[0]
-            if index >= steps:
+            number = progress[0]
+            if number >= len(events):
                 return
-            if index == gv_steps - 2:
-                for way in range(2):
-                    ring_copy(way, gv_steps).start()
-                twin_copy(piece_ref(chip, None, 0, 0), 1).start()
-            for way in range(2):
-                arrived(way, index)
-            progress[0] = index + 1
-
-    for index in range(2):
-        for way in range(2):
-            ring_copy(way, index).start()
-    twin_copy(wgv.at[own_rows, :], 0).start()
+            if number == per_stage - 2:
+                ring_start(1, 0)
+                ring_start(1, 1)
+                twin_copy(wd.at[own_rows, :], 1).start()
+            event(*events[number])
+            progress[0] = number + 1
 
     mix_load.wait()
     for g in range(groups):
         jump_loads[g].wait()
     xpad[pl.ds(8, length), :] = mixb[...].astype(jnp.float32)
-    halo_copy.wait_recv()
-    edge = halo[...].astype(jnp.float32)[8:, :]
-    xpad[pl.ds(0, 8), :] = jnp.where(sp > 0, edge, 0.0)
     taps = mix_kernel[...].astype(jnp.float32)
+    coef = -GATE_SCALE * softplus(-decay_param[...])
     chunk = 64
 
     def gates(i):
@@ -307,8 +312,33 @@
             a_s[g, at, :] = decay
             b_s[g, at, :] = drive
 
-    pl.loop(0, length // chunk)(gates)
-    pump(1)
+    pl.loop(1, length // chunk)(gates)
+    gate_load.wait()
+    chunk2 = 176
+
+    def gate_values(i):
+        at = aligned(i * chunk2, chunk2, 16)
+        for g in range(groups):
+            gel[g, at, :] = gelu(gateb[at, g * LANES : (g + 1) * LANES].astype(jnp.float32))
+
+    pl.semaphore_wait(barrier, len(partners))
+
+    halo_copy = pltpu.make_async_remote_copy(
+        src_ref=mix_hbm.at[pl.ds(length - 16, 16), :],
+        dst_ref=halo,
+        send_sem=halo_sem.at[0],
+        recv_sem=halo_sem.at[1],
+        device_id=sp_id(after),
+        device_id_type=pl.DeviceIdType.MESH,
+    )
+    halo_copy.start()
+    pl.loop(0, length // chunk2)(gate_values)
+    for copy in loads:
+        copy.wait()
+    halo_copy.wait_recv()
+    edge = halo[...].astype(jnp.float32)[8:, :]
+    xpad[pl.ds(0, 8), :] = jnp.where(sp > 0, edge, 0.0)
+    gates(0)
 
     stretch = length // SEGMENTS
 
@@ -363,16 +393,8 @@
 
     for k in range(1, TEAM):
         team_copy(k).start()
-
-    gate_load.wait()
-    chunk2 = 176
-
-    def gate_values(i):
-        at = aligned(i * chunk2, chunk2, 16)
-        for g in range(groups):
-            gel[g, at, :] = gelu(gateb[at, g * LANES : (g + 1) * LANES].astype(jnp.float32))
-
-    pl.loop(0, length // chunk2)(gate_values)
+    ring_start(0, 0)
+    twin_copy(wgv.at[own_rows, :], 0).start()
 
     for k in range(1, TEAM):
         team_copy(k).wait_recv()
@@ -393,6 +415,7 @@
     team_total[1:2, :] = tail_a * head_b + tail_b
     for k in range(1, teams):
         far_copy(k).start()
+    ring_start(0, 1)
     pump(2)
     for k in range(1, teams):
         far_copy(k).wait_recv()
@@ -445,7 +468,7 @@
                         copies.append(copy)
                     else:
                         finish(column, value)
-                pump(pumps)
+                pump(pumps[2 * s + q])
         return copies
 
     def mix_partial(block, column):
@@ -459,7 +482,7 @@
         mixed[:, pl.ds(column, sub)] = value.astype(jnp.bfloat16)
 
     rs1_copies = reduce_scatter(
-        mix_partial, rs1_send, rs1_recv, rs1_ssem, rs1_rsem, keep_mixed, 1
+        mix_partial, rs1_send, rs1_recv, rs1_ssem, rs1_rsem, keep_mixed, (1, 1, 2, 1, 2, 1, 1, 1)
     )
     resid_load.wait()
 
@@ -513,10 +536,10 @@
         for way in range(2):
             gather_copy(way, index).start()
     for index in range(2):
+        pump(2)
         for way in range(2):
             gather_wait(way, index)
             gather_copy(way, index + 4).start()
-        pump(1)
 
     tail_copy = pltpu.make_async_remote_copy(
         src_ref=up.at[pl.ds(length, 16), :],
@@ -573,32 +596,32 @@
     def around(k):
         return lax.rem(t + k, num_tp)
 
-    pump(gv_steps - progress[0])
+    pump(first_done - progress[0])
     rival = wgv.at[pl.ds(0, chips * shard), :]
     pltpu.make_async_copy(rival, rival, twin_recv.at[0]).wait()
     up_block(around(0))
-    pump(1)
+    pump(2)
     for index in range(2, 4):
         gather_wait(0, index)
     up_block(around(num_tp - 1))
-    pump(1)
+    pump(2)
     for index in range(2, 4):
         gather_wait(1, index)
     up_block(around(1))
-    pump(1)
+    pump(2)
     act_block(around(0))
-    pump(1)
+    pump(2)
     act_block(around(1))
-    pump(1)
+    pump(2)
     for index in range(4, 6):
         for way in range(2):
             gather_wait(way, index)
     up_block(around(2))
-    pump(1)
+    pump(2)
     act_block(around(2))
-    pump(1)
+    pump(2)
     act_block(around(num_tp - 1))
-    pump(steps)
+    pump(len(events))
     rival = wd.at[pl.ds(0, chips * shard), :]
     pltpu.make_async_copy(rival, rival, twin_recv.at[1]).wait()
 
@@ -611,7 +634,7 @@
         )
 
     rs2_copies = reduce_scatter(
-        down_partial, rs2_send, rs2_recv, rs2_ssem, rs2_rsem, keep_mixed, 0
+        down_partial, rs2_send, rs2_recv, rs2_ssem, rs2_rsem, keep_mixed, (0,) * 8
     )
 
     def last_rows(i):
@@ -628,9 +651,12 @@
         team_copy(k).wait_send()
     for k in range(1, teams):
         far_copy(k).wait_send()
-    for index in range(steps):
+    for stage in range(2):
         for way in range(2):
-            ring_copy(way, index).wait_send()
+            for index in range(per_stage):
+                ring_copy(way, stage, index).wait_send()
+            for distance in range(1, far + 1 - way):
+                pair_copy(way, stage, distance).wait_send()
     gathered = wgv.at[pl.ds(0, chips * shard), :]
     pltpu.make_async_copy(gathered, gathered, twin_send.at[0]).wait()
     gathered = wd.at[pl.ds(0, chips * shard), :]
@@ -669,9 +695,8 @@
     rows = length // num_tp
     sub = model // 4
     groups = channels // LANES
-    coef = (-GATE_SCALE * jax.nn.softplus(-decay_param)).reshape(1, channels)
     far = num_sp // 4
-    steps = 2 * (far - 1) + 1 + far
+    steps = 2 * (2 * far - 1)
     hbm = pl.BlockSpec(memory_space=pl.ANY)
     vmem = pl.BlockSpec(memory_space=pltpu.VMEM)
     bf16, f32 = jnp.bfloat16, jnp.float32
@@ -719,6 +744,8 @@
             dma((num_sp // TEAM - 1,)),
             dma((2, steps)),
             dma((2, steps)),
+            dma((steps,)),
+            dma((steps,)),
             dma((2,)),
             dma((2,)),
             dma(flow[:3]),
@@ -743,7 +770,7 @@
         mix_kernel,
         recur_gate_map,
         input_gate_map,
-        coef,
+        decay_param.reshape(1, channels),
         mix_gain.reshape(1, model),
         inner_gain.reshape(1, model),
         final_gain.reshape(1, model),

time: 180 us -> 158 us (0.88)
  Pallas kernels: 177 us -> 156 us
    pallas_call x1, Pallas kernels: 177 us -> 156 us  [local(): pl.pallas_call(functools.partial(layer_kernel, num_sp, num_tp), out_shape...]
where the time goes in v2:
time: 158 us
  Pallas kernels  156 us (99%)
  local copies, waits for them, and re-layouts  2.04 us (1%)
    pallas_call x1, Pallas kernels, local(): pl.pallas_call(functools.partial(layer_kernel, num_sp, num_tp), out_shape...  156 us

profile of v2, /device:TPU:33, one launch (start us, length us, event | category | flops | bytes accessed | tf_op | source)
XLA Modules:
  0.0 158.1 jit_solution(17874090342120892013)
XLA Ops:
  0.0 156.0 %shard_map.163 = bf16[176,2048]{1,0:T(8,128)(2,1)} custom-call(bf16[704,512]{1,0:T(8,128)(2,1)} %mix_hbm.1, bf16[704,512]{1,0:T(8,128)(2,1)} %gate_hbm.1, f32[704,512]{1,0:T(8,128)} %jump_hbm.1, bf16[704,2048]{1,0:T(8,128)(2,1)} %resid_hbm.1, bf16[512,2048]{1,0:T(8,128)(2,1)} %outw_hbm.1, bf16[64,1408]{1,0:T(8,128)(2,1)} %gw_hbm.1, bf16[64,1408]{1,0:T(8,128)(2,1)} %vw_hbm.1, ...), custom_call_target="tpu_custom_call" | custom-call | tf_op jit(solution)/shard_map/pallas_call | solution.py:705
  156.1 2.0 %copy.19 = bf16[176,2048]{1,0:T(8,128)(2,1)} copy(bf16[176,2048]{1,0:T(8,128)(2,1)} %shard_map.163) | data formatting | bytes 1441792

commit v3 on v2

--- a/solution.py
+++ b/solution.py
@@ -75,6 +75,7 @@
     team_ab,
     team_total,
     far_ab,
+    reached,
     rs1_send,
     rs1_recv,
     rs2_send,
@@ -270,9 +271,23 @@
                 crossed(way, stage, far - 1)
             crossed(0, stage, far)
 
-    events = [(0, k) for k in range(per_stage)] + [(1, 0), (0, per_stage)]
+    def at_distance(stage, distance):
+        first = 2 * (distance - 1)
+        return [(stage, k) for k in range(first, min(first + 2, per_stage))]
+
+    lag = far // 2
+    events = []
+    for distance in range(1, far + 1):
+        events += at_distance(0, distance)
+        if distance > lag:
+            events += at_distance(1, distance - lag)
+        if distance == lag:
+            down_start = len(events)
+    events.append((0, per_stage))
     first_done = len(events)
-    events += [(1, k) for k in range(1, per_stage + 1)]
+    for distance in range(far - lag + 1, far + 1):
+        events += at_distance(1, distance)
+    events.append((1, per_stage))
     progress = [0]
 
     def pump(count):
@@ -280,7 +295,7 @@
             number = progress[0]
             if number >= len(events):
                 return
-            if number == per_stage - 2:
+            if number == down_start:
                 ring_start(1, 0)
                 ring_start(1, 1)
                 twin_copy(wd.at[own_rows, :], 1).start()
@@ -332,9 +347,10 @@
         device_id_type=pl.DeviceIdType.MESH,
     )
     halo_copy.start()
-    pl.loop(0, length // chunk2)(gate_values)
     for copy in loads:
         copy.wait()
+    ring_start(0, 0)
+    pl.loop(0, length // chunk2)(gate_values)
     halo_copy.wait_recv()
     edge = halo[...].astype(jnp.float32)[8:, :]
     xpad[pl.ds(0, 8), :] = jnp.where(sp > 0, edge, 0.0)
@@ -356,7 +372,7 @@
         return tuple(result)
 
     unit = jnp.ones((SEGMENTS, LANES), jnp.float32)
-    ends = lax.fori_loop(0, stretch, scan_step, tuple((unit, unit * 0.0) for _ in range(groups)))
+    ends = lax.fori_loop(0, stretch, scan_step, tuple((unit, unit * 0.0) for _ in range(groups)), unroll=4)
     segments = []
     for g in range(groups):
         product, state = ends[g]
@@ -393,7 +409,7 @@
 
     for k in range(1, TEAM):
         team_copy(k).start()
-    ring_start(0, 0)
+    ring_start(0, 1)
     twin_copy(wgv.at[own_rows, :], 0).start()
 
     for k in range(1, TEAM):
@@ -415,15 +431,16 @@
     team_total[1:2, :] = tail_a * head_b + tail_b
     for k in range(1, teams):
         far_copy(k).start()
-    ring_start(0, 1)
-    pump(2)
-    for k in range(1, teams):
-        far_copy(k).wait_recv()
-    carried = jnp.zeros_like(own[0:1])
+    reached[...] = jnp.zeros_like(reached)
     for k in range(teams - 1, 0, -1):
-        pair = far_ab[k - 1]
-        carried = jnp.where(k <= team, pair[0:1] * carried + pair[1:2], carried)
-    carried = head_a * carried + head_b
+
+        @pl.when(k <= team)
+        def _():
+            far_copy(k).wait_recv()
+            pair = far_ab[k - 1]
+            reached[...] = pair[0:1] * reached[...] + pair[1:2]
+
+    carried = head_a * reached[...] + head_b
 
     inflow = [
         segments[g][0] * carried[:, g * LANES : (g + 1) * LANES] + segments[g][1]
@@ -436,11 +453,10 @@
             state = a_s[g, at, :] * inflow[g] + b_s[g, at, :]
             b_s[g, at, :] = state * gel[g, at, :]
 
-    pl.loop(0, stretch)(finish_step)
+    pl.loop(0, stretch, unroll=8)(finish_step)
     for g in range(groups):
         branch[:, pl.ds(g * LANES, LANES)] = b_s[g].astype(jnp.bfloat16)
     outw_load.wait()
-    pump(1)
 
     def reduce_scatter(partial, send, recv, ssem, rsem, finish, pumps):
         copies = []
@@ -482,7 +498,7 @@
         mixed[:, pl.ds(column, sub)] = value.astype(jnp.bfloat16)
 
     rs1_copies = reduce_scatter(
-        mix_partial, rs1_send, rs1_recv, rs1_ssem, rs1_rsem, keep_mixed, (1, 1, 2, 1, 2, 1, 1, 1)
+        mix_partial, rs1_send, rs1_recv, rs1_ssem, rs1_rsem, keep_mixed, (2, 1, 2, 1, 2, 1, 2, 1)
     )
     resid_load.wait()
 
@@ -500,46 +516,45 @@
             stream.astype(jnp.float32), inner_gain
         ).astype(jnp.bfloat16)
 
-    pl.loop(0, rows // 16)(norm_rows)
-
-    order = ((0, 1, 2, 3), (2, 3, 0, 1))
+    cut = (rows // 32 + 1) * 16
+    parts = ((0, cut), (cut, rows - cut))
+    order = tuple(
+        tuple((part, side) for part in range(2) for side in (way, 1 - way))
+        + tuple((part, way) for part in range(2))
+        for way in range(2)
+    )
+
+    def gather_ref(way, index, hops):
+        part, side = order[way][index]
+        block = lax.rem(t + (num_tp - hops if way == 0 else hops), num_tp)
+        first, size = parts[part]
+        return normed.at[aligned(block * rows + first, size, 16), pl.ds(side * half, half)]
 
     def gather_copy(way, index):
-        source = 0 if index < 4 else 1
-        block = lax.rem(t + (num_tp - source if way == 0 else source), num_tp)
-        column = order[way][index % 4] * sub
-        ref = normed.at[aligned(block * rows, rows, 16), pl.ds(column, sub)]
-        return pltpu.make_async_remote_copy(
-            src_ref=ref,
-            dst_ref=ref,
-            send_sem=ag_ssem.at[way, index],
-            recv_sem=ag_rsem.at[way, index],
-            device_id=tp_id(t_next[way]),
-            device_id_type=pl.DeviceIdType.MESH,
-        )
+        ref = gather_ref(way, index, 0 if index < 4 else 1)
+        return remote(ref, ag_ssem.at[way, index], ag_rsem.at[way, index], tp_id(t_next[way]))
 
     def gather_wait(way, index):
-        source = 1 if index < 4 else 2
-        block = lax.rem(t + (num_tp - source if way == 0 else source), num_tp)
-        column = order[way][index % 4] * sub
-        ref = normed.at[aligned(block * rows, rows, 16), pl.ds(column, sub)]
-        pltpu.make_async_remote_copy(
-            src_ref=ref,
-            dst_ref=ref,
-            send_sem=ag_ssem.at[way, index],
-            recv_sem=ag_rsem.at[way, index],
-            device_id=tp_id(t_next[way]),
-            device_id_type=pl.DeviceIdType.MESH,
+        ref = gather_ref(way, index, 1 if index < 4 else 2)
+        remote(
+            ref, ag_ssem.at[way, index], ag_rsem.at[way, index], tp_id(t_next[way])
         ).wait_recv()
 
-    for index in range(4):
-        for way in range(2):
-            gather_copy(way, index).start()
-    for index in range(2):
-        pump(2)
-        for way in range(2):
-            gather_wait(way, index)
-            gather_copy(way, index + 4).start()
+    for part in range(2):
+        first, size = parts[part]
+        pl.loop(first // 16, (first + size) // 16, unroll=size // 16)(norm_rows)
+        for index in range(2 * part, 2 * part + 2):
+            for way in range(2):
+                gather_copy(way, index).start()
+    pump(3)
+    for way in range(2):
+        gather_wait(way, 0)
+        gather_copy(way, 4).start()
+    pump(3)
+    for way in range(2):
+        gather_wait(way, 1)
+        gather_wait(way, 2)
+        gather_copy(way, 5).start()
 
     tail_copy = pltpu.make_async_remote_copy(
         src_ref=up.at[pl.ds(length, 16), :],
@@ -560,7 +575,7 @@
                 normed[source, :], wgv[:, columns], preferred_element_type=jnp.float32
             ).astype(jnp.bfloat16)
 
-        pl.loop(0, tiles)(tile)
+        pl.loop(0, tiles, unroll=tiles)(tile)
 
         @pl.when(block == num_tp - 1)
         def _():
@@ -601,26 +616,21 @@
     pltpu.make_async_copy(rival, rival, twin_recv.at[0]).wait()
     up_block(around(0))
     pump(2)
-    for index in range(2, 4):
-        gather_wait(0, index)
+    gather_wait(0, 3)
     up_block(around(num_tp - 1))
     pump(2)
-    for index in range(2, 4):
-        gather_wait(1, index)
+    gather_wait(1, 3)
     up_block(around(1))
     pump(2)
     act_block(around(0))
-    pump(2)
     act_block(around(1))
-    pump(2)
+    pump(1)
     for index in range(4, 6):
         for way in range(2):
             gather_wait(way, index)
     up_block(around(2))
-    pump(2)
+    act_block(around(num_tp - 1))
     act_block(around(2))
-    pump(2)
-    act_block(around(num_tp - 1))
     pump(len(events))
     rival = wd.at[pl.ds(0, chips * shard), :]
     pltpu.make_async_copy(rival, rival, twin_recv.at[1]).wait()
@@ -643,7 +653,7 @@
         stream += scaled(mixed[at, :].astype(jnp.float32), final_gain)
         out_ref[at, :] = stream.astype(jnp.bfloat16)
 
-    pl.loop(0, rows // 16)(last_rows)
+    pl.loop(0, rows // 16, unroll=rows // 16)(last_rows)
 
     halo_copy.wait_send()
     tail_copy.wait_send()
@@ -651,6 +661,11 @@
         team_copy(k).wait_send()
     for k in range(1, teams):
         far_copy(k).wait_send()
+
+        @pl.when(k > team)
+        def _():
+            far_copy(k).wait_recv()
+
     for stage in range(2):
         for way in range(2):
             for index in range(per_stage):
@@ -725,6 +740,7 @@
             pltpu.VMEM((TEAM - 1, 2, channels), f32),
             pltpu.VMEM((2, channels), f32),
             pltpu.VMEM((num_sp // TEAM - 1, 2, channels), f32),
+            pltpu.VMEM((1, channels), f32),
             pltpu.VMEM(flow, bf16),
             pltpu.VMEM(flow, bf16),
             pltpu.VMEM(flow, bf16),

time: 158 us -> 150 us (0.949)
  Pallas kernels: 156 us -> 148 us
    pallas_call x1, Pallas kernels: 156 us -> 148 us  [local(): pl.pallas_call(functools.partial(layer_kernel, num_sp, num_tp), out_shape...]
where the time goes in v3:
time: 150 us
  Pallas kernels  148 us (99%)
  local copies, waits for them, and re-layouts  2.04 us (1%)
    pallas_call x1, Pallas kernels, local(): pl.pallas_call(functools.partial(layer_kernel, num_sp, num_tp), out_shape...  148 us

profile of v3, /device:TPU:33, one launch (start us, length us, event | category | flops | bytes accessed | tf_op | source)
XLA Modules:
  0.0 149.8 jit_solution(9130816652028022760)
XLA Ops:
  0.0 147.7 %shard_map.163 = bf16[176,2048]{1,0:T(8,128)(2,1)} custom-call(bf16[704,512]{1,0:T(8,128)(2,1)} %mix_hbm.1, bf16[704,512]{1,0:T(8,128)(2,1)} %gate_hbm.1, f32[704,512]{1,0:T(8,128)} %jump_hbm.1, bf16[704,2048]{1,0:T(8,128)(2,1)} %resid_hbm.1, bf16[512,2048]{1,0:T(8,128)(2,1)} %outw_hbm.1, bf16[64,1408]{1,0:T(8,128)(2,1)} %gw_hbm.1, bf16[64,1408]{1,0:T(8,128)(2,1)} %vw_hbm.1, ...), custom_call_target="tpu_custom_call" | custom-call | tf_op jit(solution)/shard_map/pallas_call | solution.py:720
  147.7 2.0 %copy.19 = bf16[176,2048]{1,0:T(8,128)(2,1)} copy(bf16[176,2048]{1,0:T(8,128)(2,1)} %shard_map.163) | data formatting | bytes 1441792

commit v4 on v3

--- a/solution.py
+++ b/solution.py
@@ -80,6 +80,7 @@
     rs1_recv,
     rs2_send,
     rs2_recv,
+    ahead,
     mixed,
     hidden,
     normed,
@@ -275,7 +276,7 @@
         first = 2 * (distance - 1)
         return [(stage, k) for k in range(first, min(first + 2, per_stage))]
 
-    lag = far // 2
+    lag = far - 3
     events = []
     for distance in range(1, far + 1):
         events += at_distance(0, distance)
@@ -411,6 +412,7 @@
         team_copy(k).start()
     ring_start(0, 1)
     twin_copy(wgv.at[own_rows, :], 0).start()
+    pump(1)
 
     for k in range(1, TEAM):
         team_copy(k).wait_recv()
@@ -431,6 +433,7 @@
     team_total[1:2, :] = tail_a * head_b + tail_b
     for k in range(1, teams):
         far_copy(k).start()
+    pump(2)
     reached[...] = jnp.zeros_like(reached)
     for k in range(teams - 1, 0, -1):
 
@@ -441,6 +444,7 @@
             reached[...] = pair[0:1] * reached[...] + pair[1:2]
 
     carried = head_a * reached[...] + head_b
+    pump(1)
 
     inflow = [
         segments[g][0] * carried[:, g * LANES : (g + 1) * LANES] + segments[g][1]
@@ -459,17 +463,20 @@
     outw_load.wait()
 
     def reduce_scatter(partial, send, recv, ssem, rsem, finish, pumps):
-        copies = []
+        copies = {}
+
+        def term(s, q, way):
+            shift = num_tp - 1 - s if way == 0 else 1 + s
+            return partial(lax.rem(t + shift, num_tp), way * half + q * sub)
+
         for s in range(num_tp):
             for q in range(2):
                 for way in range(2):
-                    shift = num_tp - 1 - s if way == 0 else 1 + s
-                    block = lax.rem(t + shift, num_tp)
-                    column = way * half + q * sub
-                    value = partial(block, column)
-                    if s > 0:
-                        copies[4 * (s - 1) + 2 * q + way].wait_recv()
-                        value = value + recv[way, s - 1, q].astype(jnp.float32)
+                    if s == 0:
+                        value = term(s, q, way)
+                    else:
+                        copies[s - 1, q, way].wait_recv()
+                        value = ahead[way, q] + recv[way, s - 1, q].astype(jnp.float32)
                     if s < num_tp - 1:
                         send[way, s, q] = value.astype(jnp.bfloat16)
                         copy = pltpu.make_async_remote_copy(
@@ -481,11 +488,14 @@
                             device_id_type=pl.DeviceIdType.MESH,
                         )
                         copy.start()
-                        copies.append(copy)
+                        copies[s, q, way] = copy
                     else:
-                        finish(column, value)
+                        finish(way * half + q * sub, value)
+                if s < num_tp - 1:
+                    for way in range(2):
+                        ahead[way, q] = term(s + 1, q, way)
                 pump(pumps[2 * s + q])
-        return copies
+        return list(copies.values())
 
     def mix_partial(block, column):
         return jnp.dot(
@@ -498,7 +508,7 @@
         mixed[:, pl.ds(column, sub)] = value.astype(jnp.bfloat16)
 
     rs1_copies = reduce_scatter(
-        mix_partial, rs1_send, rs1_recv, rs1_ssem, rs1_rsem, keep_mixed, (2, 1, 2, 1, 2, 1, 2, 1)
+        mix_partial, rs1_send, rs1_recv, rs1_ssem, rs1_rsem, keep_mixed, (1, 2, 1, 2, 1, 2, 1, 1)
     )
     resid_load.wait()
 
@@ -546,7 +556,7 @@
         for index in range(2 * part, 2 * part + 2):
             for way in range(2):
                 gather_copy(way, index).start()
-    pump(3)
+    pump(4)
     for way in range(2):
         gather_wait(way, 0)
         gather_copy(way, 4).start()
@@ -565,14 +575,48 @@
         device_id_type=pl.DeviceIdType.MESH,
     )
 
-    def up_block(block):
-        source = aligned(block * rows, rows, 16)
-        target = aligned(16 + block * rows, rows, 16)
+    def act_ready(block):
+        @pl.when(block == 0)
+        def _():
+            tail_copy.wait_recv()
+
+            @pl.when(sp == 0)
+            def _():
+                up[pl.ds(0, 16), :] = jnp.zeros((16, 2 * width), jnp.bfloat16)
+
+    def act_tile(block, j):
+        columns = aligned(j * LANES, LANES, LANES)
+        results = []
+        for side, kernel in enumerate((gate_kernel, value_kernel)):
+            start = (2 * j + side) * LANES
+            value = up[
+                aligned(block * rows, rows + 16, 16), aligned(start, LANES, LANES)
+            ].astype(jnp.float32)
+            tap = kernel[:, columns].astype(jnp.float32)
+            total = value[16:] * tap[2:3]
+            for back in range(1, 3):
+                total += pltpu.roll(value, back, 0)[16:] * tap[2 - back : 3 - back]
+            results.append(total)
+        act[aligned(block * rows, rows, 16), columns] = (gelu(results[0]) * results[1]).astype(
+            jnp.bfloat16
+        )
+
+    def act_block(block):
+        act_ready(block)
+        pl.loop(0, tiles)(lambda j: act_tile(block, j))
+
+    def up_block(block, beside=None):
+        if beside is not None:
+            act_ready(beside)
 
         def tile(j):
             columns = aligned(j * 2 * LANES, 2 * LANES, LANES)
-            up[target, columns] = jnp.dot(
-                normed[source, :], wgv[:, columns], preferred_element_type=jnp.float32
+            if beside is not None:
+                act_tile(beside, j)
+            up[aligned(16 + block * rows, rows, 16), columns] = jnp.dot(
+                normed[aligned(block * rows, rows, 16), :],
+                wgv[:, columns],
+                preferred_element_type=jnp.float32,
             ).astype(jnp.bfloat16)
 
         pl.loop(0, tiles, unroll=tiles)(tile)
@@ -580,33 +624,6 @@
         @pl.when(block == num_tp - 1)
         def _():
             tail_copy.start()
-
-    def act_block(block):
-        @pl.when(block == 0)
-        def _():
-            tail_copy.wait_recv()
-
-            @pl.when(sp == 0)
-            def _():
-                up[pl.ds(0, 16), :] = jnp.zeros((16, 2 * width), jnp.bfloat16)
-
-        window = aligned(block * rows, rows + 16, 16)
-        target = aligned(block * rows, rows, 16)
-
-        def tile(j):
-            columns = aligned(j * LANES, LANES, LANES)
-            results = []
-            for side, kernel in enumerate((gate_kernel, value_kernel)):
-                start = (2 * j + side) * LANES
-                value = up[window, aligned(start, LANES, LANES)].astype(jnp.float32)
-                tap = kernel[:, columns].astype(jnp.float32)
-                total = value[16:] * tap[2:3]
-                for back in range(1, 3):
-                    total += pltpu.roll(value, back, 0)[16:] * tap[2 - back : 3 - back]
-                results.append(total)
-            act[target, columns] = (gelu(results[0]) * results[1]).astype(jnp.bfloat16)
-
-        pl.loop(0, tiles)(tile)
 
     def around(k):
         return lax.rem(t + k, num_tp)
@@ -623,12 +640,12 @@
     up_block(around(1))
     pump(2)
     act_block(around(0))
-    act_block(around(1))
-    pump(1)
+    pump(2)
     for index in range(4, 6):
         for way in range(2):
             gather_wait(way, index)
-    up_block(around(2))
+    up_block(around(2), around(1))
+    pump(1)
     act_block(around(num_tp - 1))
     act_block(around(2))
     pump(len(events))
@@ -745,6 +762,7 @@
             pltpu.VMEM(flow, bf16),
             pltpu.VMEM(flow, bf16),
             pltpu.VMEM(flow, bf16),
+            pltpu.VMEM((2, 2, rows, sub), f32),
             pltpu.VMEM((rows, model), bf16),
             pltpu.VMEM((rows, model), bf16),
             pltpu.VMEM((length, model), bf16),

time: 150 us -> 142 us (0.947)
  Pallas kernels: 148 us -> 140 us
    pallas_call x1, Pallas kernels: 148 us -> 140 us  [local(): pl.pallas_call(functools.partial(layer_kernel, num_sp, num_tp), out_shape...]
where the time goes in v4:
time: 142 us
  Pallas kernels  140 us (99%)
  local copies, waits for them, and re-layouts  2.04 us (1%)
    pallas_call x1, Pallas kernels, local(): pl.pallas_call(functools.partial(layer_kernel, num_sp, num_tp), out_shape...  140 us

profile of v4, /device:TPU:33, one launch (start us, length us, event | category | flops | bytes accessed | tf_op | source)
XLA Modules:
  0.0 141.7 jit_solution(7464725824940189583)
XLA Ops:
  0.0 139.6 %shard_map.163 = bf16[176,2048]{1,0:T(8,128)(2,1)} custom-call(bf16[704,512]{1,0:T(8,128)(2,1)} %mix_hbm.1, bf16[704,512]{1,0:T(8,128)(2,1)} %gate_hbm.1, f32[704,512]{1,0:T(8,128)} %jump_hbm.1, bf16[704,2048]{1,0:T(8,128)(2,1)} %resid_hbm.1, bf16[512,2048]{1,0:T(8,128)(2,1)} %outw_hbm.1, bf16[64,1408]{1,0:T(8,128)(2,1)} %gw_hbm.1, bf16[64,1408]{1,0:T(8,128)(2,1)} %vw_hbm.1, ...), custom_call_target="tpu_custom_call" | custom-call | tf_op jit(solution)/shard_map/pallas_call | solution.py:737
  139.6 2.0 %copy.19 = bf16[176,2048]{1,0:T(8,128)(2,1)} copy(bf16[176,2048]{1,0:T(8,128)(2,1)} %shard_map.163) | data formatting | bytes 1441792

commit v5 on v4

--- a/solution.py
+++ b/solution.py
@@ -433,7 +433,15 @@
     team_total[1:2, :] = tail_a * head_b + tail_b
     for k in range(1, teams):
         far_copy(k).start()
-    pump(2)
+
+    early = range(progress[0], progress[0] + 3)
+    progress[0] += 3
+
+    @pl.when(team > 0)
+    def _():
+        for number in early[:2]:
+            event(*events[number])
+
     reached[...] = jnp.zeros_like(reached)
     for k in range(teams - 1, 0, -1):
 
@@ -444,7 +452,11 @@
             reached[...] = pair[0:1] * reached[...] + pair[1:2]
 
     carried = head_a * reached[...] + head_b
-    pump(1)
+
+    @pl.when(team > 0)
+    def _():
+        event(*events[early[2]])
+
 
     inflow = [
         segments[g][0] * carried[:, g * LANES : (g + 1) * LANES] + segments[g][1]
@@ -462,7 +474,7 @@
         branch[:, pl.ds(g * LANES, LANES)] = b_s[g].astype(jnp.bfloat16)
     outw_load.wait()
 
-    def reduce_scatter(partial, send, recv, ssem, rsem, finish, pumps):
+    def reduce_scatter(partial, send, recv, ssem, rsem, finish, pumps, between):
         copies = {}
 
         def term(s, q, way):
@@ -491,6 +503,8 @@
                         copies[s, q, way] = copy
                     else:
                         finish(way * half + q * sub, value)
+                if s == 0 and q == 0:
+                    between()
                 if s < num_tp - 1:
                     for way in range(2):
                         ahead[way, q] = term(s + 1, q, way)
@@ -507,8 +521,21 @@
     def keep_mixed(column, value):
         mixed[:, pl.ds(column, sub)] = value.astype(jnp.bfloat16)
 
+    def early_events():
+        @pl.when(team == 0)
+        def _():
+            for number in early:
+                event(*events[number])
+
     rs1_copies = reduce_scatter(
-        mix_partial, rs1_send, rs1_recv, rs1_ssem, rs1_rsem, keep_mixed, (1, 2, 1, 2, 1, 2, 1, 1)
+        mix_partial,
+        rs1_send,
+        rs1_recv,
+        rs1_ssem,
+        rs1_rsem,
+        keep_mixed,
+        (1, 2, 1, 2, 1, 2, 1, 1),
+        early_events,
     )
     resid_load.wait()
 
@@ -628,7 +655,7 @@
     def around(k):
         return lax.rem(t + k, num_tp)
 
-    pump(first_done - progress[0])
+    pump(first_done + 2 - progress[0])
     rival = wgv.at[pl.ds(0, chips * shard), :]
     pltpu.make_async_copy(rival, rival, twin_recv.at[0]).wait()
     up_block(around(0))
@@ -640,14 +667,13 @@
     up_block(around(1))
     pump(2)
     act_block(around(0))
-    pump(2)
+    pump(1)
     for index in range(4, 6):
         for way in range(2):
             gather_wait(way, index)
     up_block(around(2), around(1))
     pump(1)
     act_block(around(num_tp - 1))
-    act_block(around(2))
     pump(len(events))
     rival = wd.at[pl.ds(0, chips * shard), :]
     pltpu.make_async_copy(rival, rival, twin_recv.at[1]).wait()
@@ -661,7 +687,14 @@
         )
 
     rs2_copies = reduce_scatter(
-        down_partial, rs2_send, rs2_recv, rs2_ssem, rs2_rsem, keep_mixed, (0,) * 8
+        down_partial,
+        rs2_send,
+        rs2_recv,
+        rs2_ssem,
+        rs2_rsem,
+        keep_mixed,
+        (0,) * 8,
+        lambda: act_block(around(2)),
     )
 
     def last_rows(i):

time: 142 us -> 140 us (0.986)
  Pallas kernels: 140 us -> 138 us
    pallas_call x1, Pallas kernels: 140 us -> 138 us  [local(): pl.pallas_call(functools.partial(layer_kernel, num_sp, num_tp), out_shape...]
where the time goes in v5:
time: 140 us
  Pallas kernels  138 us (99%)
  local copies, waits for them, and re-layouts  2.04 us (1%)
    pallas_call x1, Pallas kernels, local(): pl.pallas_call(functools.partial(layer_kernel, num_sp, num_tp), out_shape...  138 us

profile of v5, /device:TPU:33, one launch (start us, length us, event | category | flops | bytes accessed | tf_op | source)
XLA Modules:
  0.0 139.8 jit_solution(5328248910202571382)
XLA Ops:
  0.0 137.7 %shard_map.163 = bf16[176,2048]{1,0:T(8,128)(2,1)} custom-call(bf16[704,512]{1,0:T(8,128)(2,1)} %mix_hbm.1, bf16[704,512]{1,0:T(8,128)(2,1)} %gate_hbm.1, f32[704,512]{1,0:T(8,128)} %jump_hbm.1, bf16[704,2048]{1,0:T(8,128)(2,1)} %resid_hbm.1, bf16[512,2048]{1,0:T(8,128)(2,1)} %outw_hbm.1, bf16[64,1408]{1,0:T(8,128)(2,1)} %gw_hbm.1, bf16[64,1408]{1,0:T(8,128)(2,1)} %vw_hbm.1, ...), custom_call_target="tpu_custom_call" | custom-call | tf_op jit(solution)/shard_map/pallas_call | solution.py:770
  137.8 2.0 %copy.19 = bf16[176,2048]{1,0:T(8,128)(2,1)} copy(bf16[176,2048]{1,0:T(8,128)(2,1)} %shard_map.163) | data formatting | bytes 1441792

commit v6 on v5

--- a/solution.py
+++ b/solution.py
@@ -587,11 +587,6 @@
     for way in range(2):
         gather_wait(way, 0)
         gather_copy(way, 4).start()
-    pump(3)
-    for way in range(2):
-        gather_wait(way, 1)
-        gather_wait(way, 2)
-        gather_copy(way, 5).start()
 
     tail_copy = pltpu.make_async_remote_copy(
         src_ref=up.at[pl.ds(length, 16), :],
@@ -659,6 +654,10 @@
     rival = wgv.at[pl.ds(0, chips * shard), :]
     pltpu.make_async_copy(rival, rival, twin_recv.at[0]).wait()
     up_block(around(0))
+    for way in range(2):
+        gather_wait(way, 1)
+        gather_wait(way, 2)
+        gather_copy(way, 5).start()
     pump(2)
     gather_wait(0, 3)
     up_block(around(num_tp - 1))

time: 140 us -> 138 us (0.986)
  Pallas kernels: 138 us -> 136 us
    pallas_call x1, Pallas kernels: 138 us -> 136 us  [local(): pl.pallas_call(functools.partial(layer_kernel, num_sp, num_tp), out_shape...]
where the time goes in v6:
time: 138 us
  Pallas kernels  136 us (99%)
  local copies, waits for them, and re-layouts  2.04 us (1%)
    pallas_call x1, Pallas kernels, local(): pl.pallas_call(functools.partial(layer_kernel, num_sp, num_tp), out_shape...  136 us

profile of v6, /device:TPU:33, one launch (start us, length us, event | category | flops | bytes accessed | tf_op | source)
XLA Modules:
  0.0 138.1 jit_solution(4854161220126765475)
XLA Ops:
  0.0 136.1 %shard_map.163 = bf16[176,2048]{1,0:T(8,128)(2,1)} custom-call(bf16[704,512]{1,0:T(8,128)(2,1)} %mix_hbm.1, bf16[704,512]{1,0:T(8,128)(2,1)} %gate_hbm.1, f32[704,512]{1,0:T(8,128)} %jump_hbm.1, bf16[704,2048]{1,0:T(8,128)(2,1)} %resid_hbm.1, bf16[512,2048]{1,0:T(8,128)(2,1)} %outw_hbm.1, bf16[64,1408]{1,0:T(8,128)(2,1)} %gw_hbm.1, bf16[64,1408]{1,0:T(8,128)(2,1)} %vw_hbm.1, ...), custom_call_target="tpu_custom_call" | custom-call | tf_op jit(solution)/shard_map/pallas_call | solution.py:769
  136.1 2.0 %copy.19 = bf16[176,2048]{1,0:T(8,128)(2,1)} copy(bf16[176,2048]{1,0:T(8,128)(2,1)} %shard_map.163) | data formatting | bytes 1441792
